TPU v7x, 32 devices: a whole 2x2x4 slice. The times are simulated.
32 devices in a mesh: kv: 8 (over z, y), tp: 4 (over x, core).
Axes of the slice: x: 2, y: 2, z: 4, core: 2. Of those that a mesh axis runs over, the one named last changes fastest.
Arguments:
- tokens: bfloat16 [16, 16, 4096], replicated, may hold values from -6 to 6
- gain_pre: float32 [4096], replicated, may hold values from 0.1 to 1.9
- w_query: bfloat16 [4096, 2048], P('kv', 'tp'), may hold values from -0.09375 to 0.09375
- w_key: bfloat16 [4096, 2048], P('kv', 'tp'), may hold values from -0.09375 to 0.09375
- w_value: bfloat16 [4096, 2048], P('kv', 'tp'), may hold values from -0.09375 to 0.09375
- w_forget: bfloat16 [4096, 16], replicated, may hold values from -0.09375 to 0.09375
- b_forget: float32 [16], replicated
- w_out: bfloat16 [2048, 4096], P('tp', 'kv'), may hold values from -0.125 to 0.125
- gain_post: float32 [4096], P(('kv', 'tp')), may hold values from 0.1 to 1.9
- key_cache: bfloat16 [16, 1024, 16, 128], P(None, 'kv', 'tp'), may hold values from -6 to 6
- value_cache: bfloat16 [16, 1024, 16, 128], P(None, 'kv', 'tp'), may hold values from -6 to 6
- cum_cache: float32 [16, 1024, 16], P(None, 'kv', 'tp'), may hold values from -402 to 0, as said below
- lengths: int32 [16], replicated, may hold values from 512 to 992
- accepted: int32 [16], replicated, may hold values from 0 to 16
- parent: int32 [16, 16], replicated, may hold values from -1 to 14, as said below
Outputs:
- mixed: bfloat16 [16, 16, 4096], P(None, None, ('kv', 'tp'))
- key_out: bfloat16 [16, 1024, 16, 128], P(None, 'kv', 'tp')
- value_out: bfloat16 [16, 1024, 16, 128], P(None, 'kv', 'tp')
- cum_out: float32 [16, 1024, 16], P(None, 'kv', 'tp')
Inputs may be any that keep to these rules, and one draw needn't show every extreme that they name: parent[s, 0] is -1 and parent[s, i] lies between -1 and i - 1. `cum_cache`: along the positions of each sequence and head the values never rise. lengths + accepted + 16 never exceeds 1024.
All inputs are finite; a program needn't handle non-finite values.
Results may differ from a plain program's by a relative error of at most 0.03.
Values may be sent and summed in bfloat16 or wider, within the bound.
A program may use at most 64 MiB of HBM per device.

v0:
```python
import jax
import jax.numpy as jnp
from jax import lax
from jax.sharding import PartitionSpec as P

epsilon = 1e-06
floor_value = -1e30


def merged(part, axis, combine):
    gathered = jax.tree.map(lambda a: lax.all_gather(a, axis), part)

    def take(source):
        return jax.tree.map(lambda a: lax.dynamic_index_in_dim(a, source, 0, False), gathered)

    return lax.fori_loop(
        1, lax.axis_size(axis), lambda source, state: combine(state, take(source)), take(0)
    )


def ancestry(parent_ids, members):
    identity = jnp.eye(members, dtype=jnp.float32)
    parent_hot = (
        parent_ids[:, :, None] == jnp.arange(members, dtype=jnp.int32)[None, None, :]
    ).astype(jnp.float32)
    ancestors = jnp.minimum(identity[None] + parent_hot, 1.0)
    for sweep in range(max(1, (members - 1).bit_length())):
        ancestors = jnp.minimum(
            jnp.einsum("bij,bjk->bik", ancestors, ancestors, precision=lax.Precision.HIGHEST), 1.0
        )
    return ancestors


def combine_parts(first, second):
    new_max = jnp.maximum(first[0], second[0])
    first_scale = jnp.exp(first[0] - new_max)
    second_scale = jnp.exp(second[0] - new_max)
    return (
        new_max,
        first[1] * first_scale + second[1] * second_scale,
        first[2] * first_scale[..., None] + second[2] * second_scale[..., None],
        jnp.maximum(first[3], second[3]),
    )


def finish_rows(cache_max, cache_total, cache_values, last_rows, tree_max, tree_total, tree_values):
    shifted = cache_max + last_rows
    top = jnp.maximum(shifted, tree_max)
    cache_scale = jnp.exp(shifted - top)
    tree_scale = jnp.exp(tree_max - top)
    attended = (
        (cache_values * cache_scale[..., None] + tree_values * tree_scale[..., None])
        / (cache_total * cache_scale + tree_total * tree_scale)[..., None]
    ).astype(jnp.bfloat16)
    return attended.reshape(attended.shape[0], attended.shape[1] * attended.shape[2])


def per_device(
    tokens,
    gain_pre,
    w_query,
    w_key,
    w_value,
    w_forget,
    b_forget,
    w_out,
    gain_post,
    key_cache,
    value_cache,
    cum_cache,
    lengths,
    accepted,
    parent,
):
    num_seqs, proposals, model_width = tokens.shape
    kv_rank = lax.axis_index("kv")
    tp_rank = lax.axis_index("tp")
    span = key_cache.shape[1]
    heads_local = key_cache.shape[2]
    head_dim = key_cache.shape[3]
    scale = head_dim ** (-0.5)
    all_rows = num_seqs * proposals
    tok_float = tokens.astype(jnp.float32)
    normed = (
        tok_float
        * lax.rsqrt(jnp.mean(tok_float * tok_float, -1, keepdims=True) + epsilon)
        * gain_pre
    ).astype(jnp.bfloat16)
    flat = normed.reshape(all_rows, model_width)
    weight_rows = w_query.shape[0]
    local_rows = lax.dynamic_slice_in_dim(flat, kv_rank * weight_rows, weight_rows, 1)
    query_part = jnp.dot(local_rows, w_query, preferred_element_type=jnp.float32)
    key_part = jnp.dot(local_rows, w_key, preferred_element_type=jnp.float32)
    value_part = jnp.dot(local_rows, w_value, preferred_element_type=jnp.float32)
    summed = (
        lax.psum(query_part.astype(jnp.bfloat16), "kv").astype(jnp.float32),
        lax.psum(key_part.astype(jnp.bfloat16), "kv").astype(jnp.float32),
        lax.psum(value_part.astype(jnp.bfloat16), "kv").astype(jnp.float32),
    )
    query_flat = summed[0].astype(jnp.bfloat16)
    key_flat = summed[1].astype(jnp.bfloat16)
    value_flat = summed[2].astype(jnp.bfloat16)
    query = query_flat.reshape(num_seqs, proposals, heads_local, head_dim)
    key_new = key_flat.reshape(num_seqs, proposals, heads_local, head_dim)
    value_new = value_flat.reshape(num_seqs, proposals, heads_local, head_dim)
    forget_cols = lax.dynamic_slice_in_dim(w_forget, tp_rank * heads_local, heads_local, 1)
    forget_bias = lax.dynamic_slice_in_dim(b_forget, tp_rank * heads_local, heads_local, 0)
    log_forget = jax.nn.log_sigmoid(
        jnp.dot(flat, forget_cols, preferred_element_type=jnp.float32) + forget_bias
    ).reshape(num_seqs, proposals, heads_local)
    ancestors = ancestry(parent, proposals)
    path = jnp.einsum("bij,bjh->bih", ancestors, log_forget, precision=lax.Precision.HIGHEST)
    valid = lengths + accepted
    positions = kv_rank * span + jnp.arange(span, dtype=jnp.int32)
    live = (positions[None, :] < valid[:, None])[:, None, None, :]
    score = (
        jnp.einsum("bihd,bkhd->bihk", query, key_cache, preferred_element_type=jnp.float32) * scale
        + path[..., None]
        - jnp.swapaxes(cum_cache, 1, 2)[:, None]
    )
    block_max = jnp.max(jnp.where(live, score, floor_value), axis=-1)
    weight = jnp.exp(jnp.where(live, score - block_max[..., None], floor_value))
    block_total = jnp.sum(weight, axis=-1)
    block_values = jnp.einsum(
        "bihk,bkhd->bihd",
        weight.astype(jnp.bfloat16),
        value_cache,
        preferred_element_type=jnp.float32,
    )
    owner = positions[None, :] == (valid - 1)[:, None]
    candidate = jnp.max(jnp.where(owner[:, :, None], cum_cache, floor_value), axis=1)
    tree_mask = (ancestors > 0.5)[:, :, None, :]
    tree_score = (
        jnp.einsum("bihd,bjhd->bihj", query, key_new, preferred_element_type=jnp.float32) * scale
        + path[..., None]
        - jnp.swapaxes(path, 1, 2)[:, None]
    )
    tree_max = jnp.max(jnp.where(tree_mask, tree_score, floor_value), axis=-1)
    tree_weight = jnp.exp(jnp.where(tree_mask, tree_score - tree_max[..., None], floor_value))
    tree_total = jnp.sum(tree_weight, axis=-1)
    tree_values = jnp.einsum(
        "bihj,bjhd->bihd",
        tree_weight.astype(jnp.bfloat16),
        value_new,
        preferred_element_type=jnp.float32,
    )
    tree_max_rows = tree_max.reshape(all_rows, heads_local)
    tree_total_rows = tree_total.reshape(all_rows, heads_local)
    tree_values_rows = tree_values.reshape(all_rows, heads_local, head_dim)
    cache_max, cache_total, cache_values, last_cum = merged(
        (block_max, block_total, block_values, candidate), "kv", combine_parts
    )
    last_rows = jnp.broadcast_to(last_cum[:, None, :], (num_seqs, proposals, heads_local)).reshape(
        all_rows, heads_local
    )
    attended = finish_rows(
        cache_max.reshape(all_rows, heads_local),
        cache_total.reshape(all_rows, heads_local),
        cache_values.reshape(all_rows, heads_local, head_dim),
        last_rows,
        tree_max_rows,
        tree_total_rows,
        tree_values_rows,
    )
    mixed_part = jnp.dot(attended, w_out, preferred_element_type=jnp.float32)
    mixed_sum = lax.psum_scatter(
        mixed_part.astype(jnp.bfloat16), "tp", scatter_dimension=1, tiled=True
    ).astype(jnp.float32)
    squares = lax.psum(jnp.sum(mixed_sum * mixed_sum, axis=1), ("kv", "tp"))
    mixed = (mixed_sum * lax.rsqrt(squares / model_width + epsilon)[:, None] * gain_post).astype(
        jnp.bfloat16
    )
    mixed = mixed.reshape(num_seqs, proposals, mixed_sum.shape[1])
    relative = positions[None, :] - valid[:, None]
    select = relative[:, :, None] == jnp.arange(proposals, dtype=jnp.int32)[None, None, :]
    written = (relative >= 0) & (relative < proposals)
    placed_keys = jnp.einsum(
        "bkj,bjhd->bkhd", select.astype(jnp.bfloat16), key_new, preferred_element_type=jnp.float32
    ).astype(jnp.bfloat16)
    placed_values = jnp.einsum(
        "bkj,bjhd->bkhd", select.astype(jnp.bfloat16), value_new, preferred_element_type=jnp.float32
    ).astype(jnp.bfloat16)
    key_out = jnp.where(written[:, :, None, None], placed_keys, key_cache)
    value_out = jnp.where(written[:, :, None, None], placed_values, value_cache)
    cum_new = last_cum[:, None, :] + path
    placed_cum = jnp.einsum(
        "bkj,bjh->bkh", select.astype(jnp.float32), cum_new, precision=lax.Precision.HIGHEST
    )
    cum_out = jnp.where(written[:, :, None], placed_cum, cum_cache)
    return (mixed, key_out, value_out, cum_out)


def solution(mesh):
    return jax.shard_map(
        per_device,
        mesh=mesh,
        in_specs=(
            P(),
            P(),
            P("kv", "tp"),
            P("kv", "tp"),
            P("kv", "tp"),
            P(),
            P(),
            P("tp", "kv"),
            P(("kv", "tp")),
            P(None, "kv", "tp", None),
            P(None, "kv", "tp", None),
            P(None, "kv", "tp"),
            P(),
            P(),
            P(),
        ),
        out_specs=(
            P(None, None, ("kv", "tp")),
            P(None, "kv", "tp", None),
            P(None, "kv", "tp", None),
            P(None, "kv", "tp"),
        ),
        check_vma=False,
    )
```

profile of v0, /device:TPU:0, one launch (start us, length us, event | category | flops | bytes accessed | tf_op | source)
XLA Modules:
  0.0 293.7 jit_solution(18166977951993972896)
XLA Ops:
  7.2 2.1 fusion.4
  9.4 2.2 fusion.6
  12.8 1.3 convolution_convert_fusion.1
  14.2 1.4 convolution_convert_fusion.3
  18.0 1.5 fusion.71
  20.6 75.1 %all-reduce.3.cloned.1.call-done = (bf16[16,16,4,128]{3,1,2,0:T(8,128)(2,1)}, bf16[16,16,4,128]{3,1,2,0:T(8,128)(2,1)}, bf16[16,16,4,128]{3,1,2,0:T(8,128)(2,1)}) async-done(((bf16[16,16,4,128]{3,1,2,0:T(8,128)(2,1)}, bf16[16,16,4,128]{3,1,2,0:T(8,128)(2,1)}, bf16[16,16,4,128]{3,1,2,0:T(8,128)(2,1)}), (bf16[16,16,4,128]{3,1,2,0:T(8,128)(2,1)}, bf16[16,16,4,128]{3,1,2,0:T(8,128)(2,1)}, ...) | async-done | bytes 786448 | tf_op jit(solution)/shard_map/psum | solution.py:97
  95.7 3.0 %select_reduce_fusion.1 = (f32[16,16,4]{1,2,0:T(4,128)S(1)}, f32[16,16,4,128]{3,1,2,0:T(8,128)S(1)}) fusion(pred[16,128]{1,0:T(8,128)(4,1)S(1)} %get-tuple-element.314, f32[16,4,128]{2,1,0:T(4,128)S(1)} %bitcast.132, f32[16,16,4]{1,2,0:T(4,128)S(1)} %fusion.63, bf16[16,16,4,128]{3,1,2,0:T(8,128)(2,1)} %get-tuple-element.302, ...), kind=kOutput, calls=%fused_computation.51 | convolution fusion | flops 34208768 | bytes 2926592 | tf_op jit(solution)/shard_map/bihd,bkhd->bihk/dot_general | solution.py:117
  99.5 1.5 fusion.11
  101.4 26.7 %all-gather.4 = f32[8,16,4]{1,2,0:T(4,128)S(1)} all-gather(f32[1,16,4]{1,2,0:T(4,128)S(1)} %bitcast.134), channel_id=5, replica_groups=mesh['kv'=8,'tp'=4] {'kv'}, dimensions={0}, use_global_device_ids=true | all-gather | bytes 2304 | tf_op jit(solution)/shard_map/all_gather | solution.py:11
  128.8 1.4 select_reduce_fusion
  131.9 32.2 %all-gather = f32[128,16,4]{1,2,0:T(4,128)S(1)} all-gather(f32[16,16,4]{1,2,0:T(4,128)S(1)} %get-tuple-element.320), channel_id=2, replica_groups=mesh['kv'=8,'tp'=4] {'kv'}, dimensions={0}, use_global_device_ids=true | all-gather | bytes 36864 | tf_op jit(solution)/shard_map/all_gather | solution.py:11
  164.1 1.5 fusion.33
  165.6 31.7 %all-gather.1 = f32[128,16,4]{1,2,0:T(4,128)S(1)} all-gather(f32[16,16,4]{1,2,0:T(4,128)S(1)} %fusion.33), channel_id=3, replica_groups=mesh['kv'=8,'tp'=4] {'kv'}, dimensions={0}, use_global_device_ids=true | all-gather | bytes 36864 | tf_op jit(solution)/shard_map/all_gather | solution.py:11
  198.3 3.1 %copy.110 = bf16[16,128,4,128]{3,2,1,0:T(4,128)(2,1)} copy(bf16[16,128,4,128]{3,1,2,0:T(8,128)(2,1)S(1)} %convert_select_fusion) | data formatting | bytes 4194304
  202.6 22.1 %while.21 = (s32[]{:T(128)}, f32[16,16,4]{1,2,0:T(4,128)S(1)}, f32[16,16,4]{1,2,0:T(4,128)S(1)}, f32[16,16,4,128]{3,2,1,0:T(4,128)S(1)}, f32[16,4]{0,1:T(4,128)S...) while((s32[]{:T(128)}, f32[16,16,4]{1,2,0:T(4,128)S(1)}, ...), condition=%wide.region_6.7_spmd, body=%wide.region_5.6_spmd.sunk | while | flops 399429 | bytes 2679715 | solution.py:16
  203.8 1.1 constant_dynamic-slice_fusion.2
  206.9 1.1 constant_dynamic-slice_fusion.2
  210.1 1.1 constant_dynamic-slice_fusion.2
  213.2 1.1 constant_dynamic-slice_fusion.2
  216.4 1.1 constant_dynamic-slice_fusion.2
  227.8 2.4 convert_select_fusion.1
  230.2 3.1 %copy.109 = bf16[16,128,4,128]{3,2,1,0:T(4,128)(2,1)} copy(bf16[16,128,4,128]{3,1,2,0:T(8,128)(2,1)S(1)} %convert_select_fusion.1) | data formatting | bytes 4194304
  234.2 11.8 %reduce-scatter.4.cloned.1.call-done = bf16[128,256]{1,0:T(8,128)(2,1)} async-done(((bf16[512,256]{1,0:T(8,128)(2,1)}), bf16[128,256]{1,0:T(8,128)(2,1)}) %reduce-scatter.4.cloned.1.call-update) | async-done | bytes 65552
  247.1 39.3 %psum.31 = f32[256]{0:T(256)S(1)} all-reduce(f32[256]{0:T(256)S(1)} %fusion.48), channel_id=1, replica_groups=mesh['kv'=8,'tp'=4] {'kv','tp'}, use_global_device_ids=true, to_apply=%region_13.14 | all-reduce | flops 256 | bytes 2048 | tf_op jit(solution)/shard_map/psum | solution.py:169
  (138 shorter events, 32.6 us)
Async XLA Ops:
  7.2 4.5 %copy-start = (bf16[512,512]{1,0:T(8,128)(2,1)S(1)}, bf16[512,512]{1,0:T(8,128)(2,1)}, u32[]{:S(2)}) copy-start(bf16[512,512]{1,0:T(8,128)(2,1)} %param.20) | copy-start | bytes 1572868
  7.2 2.2 copy-start.10
  7.2 88.5 %all-reduce.3.cloned.1.call-start = ((), (), s32[]{:S(2)}) async-start(), calls=%async_computation.3 | async-start | bytes 1572864 | tf_op jit(solution)/shard_map/psum | solution.py:97
  14.1 3.2 %copy-start.17 = (s32[16,16]{1,0:T(8,128)S(1)}, s32[16,16]{1,0:T(8,128)}, u32[]{:S(2)}) copy-start(s32[16,16]{1,0:T(8,128)} %param.31) | copy-start | bytes 3076
  14.1 3.8 %copy-start.18 = (f32[16]{0:T(128)S(1)}, f32[16]{0:T(128)}, u32[]{:S(2)}) copy-start(f32[16]{0:T(128)} %param.23) | copy-start | bytes 196
  14.1 3.9 %copy-start.13 = (s32[16]{0:T(128)S(1)}, s32[16]{0:T(128)}, u32[]{:S(2)}) copy-start(s32[16]{0:T(128)} %param.29) | copy-start | bytes 196
  14.1 3.9 %copy-start.14 = (s32[16]{0:T(128)S(1)}, s32[16]{0:T(128)}, u32[]{:S(2)}) copy-start(s32[16]{0:T(128)} %param.30) | copy-start | bytes 196
  17.2 78.5 %copy-start.6 = (f32[16,128,4]{1,2,0:T(4,128)S(1)}, f32[16,128,4]{1,2,0:T(4,128)}, u32[]{:S(2)}) copy-start(f32[16,128,4]{1,2,0:T(4,128)} %param.28) | copy-start | bytes 98308
  17.2 184.2 %all-gather.7.cloned.1.call-start = ((), (), s32[]{:S(2)}) async-start(), calls=%async_computation.1 | async-start | bytes 4718592 | tf_op jit(solution)/shard_map/all_gather | solution.py:11
  19.7 79.8 %copy-start.1 = (bf16[16,128,4,128]{3,2,1,0:T(4,128)(2,1)S(1)}, bf16[16,128,4,128]{3,2,1,0:T(4,128)(2,1)}, u32[]{:S(2)}) copy-start(bf16[16,128,4,128]{3,2,1,0:T(4,128)(2,1)} %param.27) | copy-start | bytes 6291460
  20.5 108.2 %copy-start.8 = (f32[16,16,4]{1,2,0:T(4,128)}, f32[16,16,4]{1,2,0:T(4,128)S(1)}, u32[]{:S(2)}) copy-start(f32[16,16,4]{1,2,0:T(4,128)S(1)} %fusion.63) | copy-start | bytes 12292
  98.7 0.8 copy-start.2
  99.5 30.7 %copy-start.4 = (bf16[16,16,4,128]{3,1,2,0:T(8,128)(2,1)S(1)}, bf16[16,16,4,128]{3,1,2,0:T(8,128)(2,1)}, u32[]{:S(2)}) copy-start(bf16[16,16,4,128]{3,1,2,0:T(8,128)(2,1)} %get-tuple-element.303) | copy-start | bytes 786436
  101.0 144.9 %reduce-scatter.4.cloned.1.call-start = ((), (), s32[]{:S(2)}) async-start(), calls=%async_computation.2 | async-start | bytes 327680
  128.1 0.7 copy-start.5
  130.2 67.0 %copy-start.11 = (s32[16,128]{1,0:T(8,128)S(1)}, s32[16,128]{1,0:T(8,128)}, u32[]{:S(2)}) copy-start(s32[16,128]{1,0:T(8,128)} %broadcast_subtract_fusion) | copy-start | bytes 24580
  224.7 1.9 copy-start.3
  224.8 1.8 copy-start.15
  226.6 1.2 copy-start.16
  230.2 3.1 %copy-start.7 = (f32[16,128,4]{1,2,0:T(4,128)S(1)}, f32[16,128,4]{1,2,0:T(4,128)}, u32[]{:S(2)}) copy-start(f32[16,128,4]{1,2,0:T(4,128)} %param.28) | copy-start | bytes 98308
  230.2 3.1 %copy-start.9 = (f32[16,16,4]{1,2,0:T(4,128)S(1)}, f32[16,16,4]{1,2,0:T(4,128)}, u32[]{:S(2)}) copy-start(f32[16,16,4]{1,2,0:T(4,128)} %copy-done.8) | copy-start | bytes 12292
  230.2 56.1 %copy-start.12 = (f32[128]{0:T(128)S(1)}, f32[128]{0:T(128)}, u32[]{:S(2)}) copy-start(f32[128]{0:T(128)} %param.25) | copy-start | bytes 1540
Sparse Core Ops, SparseCore 0:
  17.3 78.3 all-reduce.2
  101.2 77.8 all-gather.6
  228.0 17.9 reduce-scatter.3
where the time goes:
time: 295 us; the launch traced here: 294 us
  blocking collectives  130 us (44%)
  waiting for transfers between devices  87 us (29%)
  local copies, waits for them, and re-layouts  25.7 us (9%)
  other arithmetic  19.7 us (7%)
  matrix products  16.7 us (6%)
  between operations  14.2 us (5%)
    all_gather x3, blocking collectives, merged(): gathered = jax.tree.map(lambda a: lax.all_gather(a, axis), part)  90.6 us
    psum x1, waiting for transfers between devices, per_device(): lax.psum(key_part.astype(jnp.bfloat16), 'kv').astype(jnp.float32)  75.1 us
    psum x1, blocking collectives, per_device(): squares = lax.psum(jnp.sum(mixed_sum * mixed_sum, axis=1), ('kv', 'tp'))  39.3 us
    unnamed x4, waiting for transfers between devices  11.8 us
    unnamed x42, local copies, waits for them, and re-layouts  8.8 us
    dynamic_slice x11, local copies, waits for them, and re-layouts, take(): lax.dynamic_index_in_dim(a, source, 0, False)  8.64 us
    add x7, other arithmetic, combine_parts(): first[2] * first_scale[..., None] + second[2] * second_scale[..., None]  6.66 us
  transfers between devices with their start and end apart: 3, of which 2 were waited for; matrix products, arithmetic and copies ran while one was open for 7% of the time, Pallas kernels for 0%

commit v1 on v0

--- a/solution.py
+++ b/solution.py
@@ -1,6 +1,10 @@
+import functools
+
 import jax
 import jax.numpy as jnp
 from jax import lax
+from jax.experimental import pallas as pl
+from jax.experimental.pallas import tpu as pltpu
 from jax.sharding import PartitionSpec as P
 
 epsilon = 1e-06
@@ -190,9 +194,649 @@
     return (mixed, key_out, value_out, cum_out)
 
 
+MESH = pl.DeviceIdType.MESH
+HI = lax.Precision.HIGHEST
+F32 = jnp.float32
+BF = jnp.bfloat16
+
+
+def iota(shape, dim):
+    return lax.broadcasted_iota(jnp.int32, shape, dim)
+
+
+def hot(mask):
+    return jnp.where(mask, 1.0, 0.0).astype(F32)
+
+
+def dot_hi(a, b, dims=(((1,), (0,)), ((), ()))):
+    return lax.dot_general(a, b, dims, precision=HI, preferred_element_type=F32)
+
+
+NT = (((1,), (1,)), ((), ()))
+
+
+def layer_kernel(
+    n,
+    nt,
+    num_seqs,
+    prop,
+    heads,
+    hd,
+    span,
+    tok,
+    gain,
+    wq,
+    wk,
+    wv,
+    wft,
+    bias,
+    wo,
+    gpost,
+    kc,
+    vc,
+    cum,
+    lens,
+    accs,
+    parent,
+    mixed_out,
+    k_out,
+    v_out,
+    cum_out,
+    tokv,
+    normed,
+    wv3,
+    wov,
+    kcv,
+    vcv,
+    part,
+    rs_recv,
+    qkv,
+    st_send,
+    val_send,
+    st_recv,
+    val_recv,
+    cand_send,
+    cand_recv,
+    brow,
+    anc,
+    tpath,
+    ptile,
+    att,
+    o_send,
+    o_recv,
+    sq_send,
+    sq_recv,
+    sq2_send,
+    sq2_recv,
+    loc,
+    ssem,
+    rsem,
+    tssem,
+    trsem,
+):
+    me = lax.axis_index("kv")
+    mt = lax.axis_index("tp")
+    rows = num_seqs * prop
+    width = tok.shape[1]
+    hw = heads * hd
+    kdim = wq.shape[0]
+    cols = heads * span
+    sp = num_seqs // n
+    R = sp * prop
+    hp = heads * prop
+    L = sp * hp
+    scale = hd ** (-0.5)
+    base = me * span
+    heads_all = wft.shape[0]
+
+    barrier = pltpu.get_barrier_semaphore()
+
+    def greet(d, c):
+        pl.semaphore_signal(
+            barrier, inc=1, device_id={"kv": lax.rem(me + d, n)}, device_id_type=MESH
+        )
+        return c
+
+    def greet_t(d, c):
+        pl.semaphore_signal(
+            barrier, inc=1, device_id={"tp": lax.rem(mt + d, nt)}, device_id_type=MESH
+        )
+        return c
+
+    lax.fori_loop(1, n, greet, 0)
+    lax.fori_loop(1, nt, greet_t, 0)
+
+    in_tok = pltpu.make_async_copy(tok, tokv, loc.at[0])
+    in_w = [pltpu.make_async_copy(w, wv3.at[i], loc.at[1 + i]) for i, w in enumerate((wq, wk, wv))]
+    in_kc = pltpu.make_async_copy(kc, kcv, loc.at[4])
+    in_vc = pltpu.make_async_copy(vc, vcv, loc.at[5])
+    in_wo = pltpu.make_async_copy(wo, wov, loc.at[6])
+    in_tok.start()
+    for c in in_w:
+        c.start()
+    in_kc.start()
+    in_vc.start()
+    in_wo.start()
+
+    def to_kv(ph, d, src, dst, sign=1):
+        peer = lax.rem(me + sign * d + n, n)
+        return pltpu.make_async_remote_copy(
+            src_ref=src,
+            dst_ref=dst,
+            send_sem=ssem.at[ph, d],
+            recv_sem=rsem.at[ph, d],
+            device_id={"kv": peer},
+            device_id_type=MESH,
+        )
+
+    def to_tp(ph, d, src, dst):
+        peer = lax.rem(mt + d, nt)
+        return pltpu.make_async_remote_copy(
+            src_ref=src,
+            dst_ref=dst,
+            send_sem=tssem.at[ph, d],
+            recv_sem=trsem.at[ph, d],
+            device_id={"tp": peer},
+            device_id_type=MESH,
+        )
+
+    def up(d):
+        return lax.rem(me + d, n)
+
+    def down(d):
+        return lax.rem(me - d + n, n)
+
+    def rrow(i):
+        return pl.ds(pl.multiple_of(i * R, R), R)
+
+    def rs_copy(ph, d):
+        return to_kv(ph, d, part.at[ph, rrow(up(d))], rs_recv.at[ph, d])
+
+    def ag_copy(ph, d):
+        return to_kv(3 + ph, d, qkv.at[ph, rrow(me)], qkv.at[ph, rrow(me)])
+
+    def ag_wait(ph, d):
+        to_kv(3 + ph, d, qkv.at[ph, rrow(me)], qkv.at[ph, rrow(down(d))]).wait_recv()
+
+    def stat_copy(d):
+        return to_kv(6, d, st_send.at[d], st_recv.at[d], -1)
+
+    def val_copy(d):
+        return to_kv(7, d, val_send.at[d], val_recv.at[d], -1)
+
+    def cand_copy(d):
+        return to_kv(8, d, cand_send, cand_recv.at[d])
+
+    def att_copy(d):
+        return to_kv(9, d, att.at[rrow(me)], att.at[rrow(me)])
+
+    def att_wait(d):
+        to_kv(9, d, att.at[rrow(me)], att.at[rrow(down(d))]).wait_recv()
+
+    def sq_copy(d):
+        return to_kv(10, d, sq_send, sq_recv.at[d])
+
+    def each(count, fn):
+        def body(d, c):
+            fn(d)
+            return c
+
+        lax.fori_loop(1, count, body, 0)
+
+    in_tok.wait()
+    nb = prop
+
+    def norm_rows(i, c):
+        sl = pl.ds(pl.multiple_of(i * nb, nb), nb)
+        t = tokv[sl, :].astype(F32)
+        inv = lax.rsqrt(jnp.mean(t * t, axis=-1, keepdims=True) + epsilon)
+        normed[sl, :] = (t * inv * gain[...]).astype(BF)
+        return c
+
+    lax.fori_loop(0, rows // nb, norm_rows, 0)
+    local = normed[:, pl.ds(pl.multiple_of(me * kdim, kdim), kdim)]
+    pl.semaphore_wait(barrier, n - 1 + nt - 1)
+    for ph in range(3):
+        in_w[ph].wait()
+        part[ph] = jnp.dot(local, wv3[ph], preferred_element_type=F32).astype(BF)
+        each(n, lambda d: rs_copy(ph, d).start())
+
+    r64 = num_seqs * heads
+    c64 = cum[...]
+    srow = iota((r64, span), 0) // heads
+    lane = iota((r64, span), 1)
+    rel64 = jnp.zeros((r64, span), jnp.int32)
+    rel16 = jnp.zeros((num_seqs, cols), jnp.int32)
+    s16 = iota((num_seqs, cols), 0)
+    for s in range(num_seqs):
+        rel_s = lens[s] + accs[s] - base
+        rel64 = jnp.where(srow == s, rel_s, rel64)
+        rel16 = jnp.where(s16 == s, rel_s, rel16)
+    cand = jnp.max(jnp.where(lane == rel64 - 1, c64, floor_value), axis=1, keepdims=True)
+    diag = iota((r64, 128), 0) == iota((r64, 128), 1)
+    cand_lane = jnp.sum(jnp.where(diag, cand, 0.0), axis=0, keepdims=True)
+    cand_send[...] = jnp.broadcast_to(cand_lane, (8, 128))
+    each(n, lambda d: cand_copy(d).start())
+
+    spread = hot(iota((span, cols), 1) // heads == iota((span, cols), 0))
+    e1 = dot_hi(c64, spread)
+    e1 = jnp.where(iota((r64, cols), 0) % heads == iota((r64, cols), 1) % heads, e1, 0.0)
+    take = hot(iota((num_seqs, r64), 1) // heads == iota((num_seqs, r64), 0))
+    cflat = dot_hi(take, e1)
+    brow[...] = jnp.where(iota((num_seqs, cols), 1) // heads < rel16, -cflat, floor_value)
+
+    ri = iota((rows, rows), 0)
+    ci = iota((rows, rows), 1)
+    pick = hot(iota((rows, num_seqs), 0) // prop == iota((rows, num_seqs), 1))
+    pb = dot_hi(pick, parent[...].astype(F32))
+    pcol = jnp.sum(
+        jnp.where(iota((rows, prop), 1) == iota((rows, prop), 0) % prop, pb, 0.0),
+        axis=1,
+        keepdims=True,
+    )
+    target = jnp.where(pcol >= 0.0, (ri // prop * prop).astype(F32) + pcol, -1.0)
+    a = jnp.where((ri == ci) | (ci.astype(F32) == target), 1.0, 0.0)
+    for sweep in range(max(1, (prop - 1).bit_length())):
+        low = a.astype(BF)
+        a = jnp.minimum(jnp.dot(low, low, preferred_element_type=F32), 1.0)
+    anc[...] = a
+    lf = lax.dot_general(wft[...], normed[...], NT, preferred_element_type=F32)
+    bcol = jnp.zeros((heads_all, rows), F32)
+    for h in range(heads_all):
+        bcol = jnp.where(iota((heads_all, rows), 0) == h, bias[h], bcol)
+    z = lf + bcol
+    lf = jnp.minimum(z, 0.0) - jnp.log1p(jnp.exp(-jnp.abs(z)))
+    path_t = dot_hi(lf, a, NT)
+    rep = hot(iota((r64, heads_all), 1) == mt * heads + iota((r64, heads_all), 0) % heads)
+    pm = dot_hi(rep, path_t)
+    pm = jnp.where(iota((r64, rows), 1) // prop == iota((r64, rows), 0) // heads, pm, 0.0)
+    fold = hot(iota((rows, 128), 0) % prop == iota((rows, 128), 1) % prop)
+    pt = dot_hi(pm, fold)
+    ptile[...] = pt
+    ptm = jnp.where((iota((r64, 128), 1) // prop) % heads == iota((r64, 128), 0) % heads, pt, 0.0)
+    tpath[...] = dot_hi(take, ptm)
+
+    def reduce_part(ph):
+        total = part[ph, rrow(me)].astype(F32)
+        for d in range(1, n):
+            rs_copy(ph, d).wait_recv()
+            total = total + rs_recv[ph, d].astype(F32)
+        qkv[ph, rrow(me)] = total.astype(BF)
+        each(n, lambda d: ag_copy(ph, d).start())
+
+    for ph in range(3):
+        reduce_part(ph)
+
+    in_kc.wait()
+    in_vc.wait()
+    same_head = iota((hp, cols), 0) // prop == iota((hp, cols), 1) % heads
+    diag_l = iota((L, L), 0) == iota((L, L), 1)
+
+    def heads_of(ph, s):
+        block = qkv[ph, pl.ds(pl.multiple_of(s * prop, prop), prop), :]
+        return jnp.concatenate([block[:, h * hd : (h + 1) * hd] for h in range(heads)], axis=0)
+
+    def block_part(src):
+        maxes, totals, values = [], [], []
+        for j in range(sp):
+            s = src * sp + j
+            q = heads_of(0, s)
+            sc = lax.dot_general(q, kcv[s], NT, preferred_element_type=F32) * scale
+            sc = jnp.where(same_head, sc + brow[pl.ds(s, 1), :], floor_value)
+            m = jnp.max(sc, axis=1, keepdims=True)
+            w = jnp.exp(sc - m)
+            maxes.append(m)
+            totals.append(jnp.sum(w, axis=1, keepdims=True))
+            values.append(
+                jnp.dot(w.astype(BF), vcv[s], preferred_element_type=F32).astype(BF)
+            )
+        m = jnp.concatenate(maxes, axis=0)
+        t = jnp.concatenate(totals, axis=0)
+        m_lane = jnp.sum(jnp.where(diag_l, m, 0.0), axis=0, keepdims=True)
+        t_lane = jnp.sum(jnp.where(diag_l, t, 0.0), axis=0, keepdims=True)
+        stats = jnp.where(iota((8, L), 0) == 0, m_lane, t_lane)
+        return stats, jnp.concatenate(values, axis=0)
+
+    def remote_block(d):
+        ag_wait(0, d)
+        stats, values = block_part(down(d))
+        st_send[d] = stats
+        val_send[d] = values
+        stat_copy(d).start()
+        val_copy(d).start()
+
+    each(n, remote_block)
+    stats, values = block_part(me)
+    st_recv[0] = stats
+    val_recv[0] = values
+
+    fold_h = iota((rows, hp), 0)
+    tmax, ttot, tval = [], [], []
+    for j in range(sp):
+        s = me * sp + j
+        q = heads_of(0, s)
+        k = heads_of(1, s)
+        v = heads_of(2, s)
+        arows = anc[pl.ds(pl.multiple_of(s * prop, prop), prop), :]
+        sel = hot(fold_h == s * prop + iota((rows, hp), 1) % prop).astype(BF)
+        am = jnp.dot(arows.astype(BF), sel, preferred_element_type=F32)
+        am = jnp.concatenate([am] * heads, axis=0)
+        mask = (am > 0.5) & (iota((hp, hp), 0) // prop == iota((hp, hp), 1) // prop)
+        sc = lax.dot_general(q, k, NT, preferred_element_type=F32) * scale
+        sc = jnp.where(mask, sc - tpath[pl.ds(s, 1), 0:hp], floor_value)
+        m = jnp.max(sc, axis=1, keepdims=True)
+        w = jnp.where(mask, jnp.exp(sc - m), 0.0)
+        tmax.append(m)
+        ttot.append(jnp.sum(w, axis=1, keepdims=True))
+        tval.append(jnp.dot(w.astype(BF), v, preferred_element_type=F32))
+    tree_max = jnp.concatenate(tmax, axis=0)
+    tree_tot = jnp.concatenate(ttot, axis=0)
+    tree_val = jnp.concatenate(tval, axis=0)
+
+    last_lane = cand_send[...]
+    for d in range(1, n):
+        cand_copy(d).wait_recv()
+        last_lane = jnp.maximum(last_lane, cand_recv[d])
+    last_col = jnp.sum(jnp.where(diag, last_lane[0:1], 0.0), axis=1, keepdims=True)
+    own_rows = iota((L, 128), 0)
+    own_pick = iota((L, 128), 1) == (me * sp + own_rows // hp) * heads + (own_rows % hp) // prop
+    last_own = jnp.sum(jnp.where(own_pick, last_lane[0:1], 0.0), axis=1, keepdims=True)
+
+    shifted_path = ptile[...]
+    for b in range((span - 1).bit_length()):
+        moved = pltpu.roll(shifted_path, 1 << b, 1)
+        shifted_path = jnp.where((rel64 >> b) & 1 == 1, moved, shifted_path)
+    off = lane - rel64
+    cum_out[...] = jnp.where((off >= 0) & (off < prop), last_col + shifted_path, cum[...])
+
+    for d in range(1, n):
+        stat_copy(d).wait_recv()
+    top = st_recv[0]
+    for d in range(1, n):
+        top = jnp.maximum(top, st_recv[d])
+    top = top[0:1]
+
+    def col(x):
+        return jnp.sum(jnp.where(diag_l, x, 0.0), axis=1, keepdims=True)
+
+    cache_tot = jnp.zeros((1, L), F32)
+    scales = []
+    for d in range(n):
+        sd = jnp.exp(st_recv[d, 0:1] - top)
+        scales.append(col(sd))
+        cache_tot = cache_tot + st_recv[d, 1:2] * sd
+    shifted = col(top) + last_own
+    both = jnp.maximum(shifted, tree_max)
+    cscale = jnp.exp(shifted - both)
+    tscale = jnp.exp(tree_max - both)
+    denom = col(cache_tot) * cscale + tree_tot * tscale
+    vals = jnp.zeros((L, hd), F32)
+    for d in range(n):
+        if d > 0:
+            val_copy(d).wait_recv()
+        vals = vals + val_recv[d].astype(F32) * scales[d]
+    attended = ((vals * cscale + tree_val * tscale) / denom).astype(BF)
+    for j in range(sp):
+        for h in range(heads):
+            att[pl.ds(pl.multiple_of(me * R + j * prop, prop), prop), h * hd : (h + 1) * hd] = (
+                attended[j * hp + h * prop : j * hp + (h + 1) * prop]
+            )
+    each(n, lambda d: att_copy(d).start())
+    each(n, lambda d: ag_wait(1, d))
+    each(n, lambda d: ag_wait(2, d))
+    out_k = pltpu.make_async_copy(qkv.at[1], k_out, loc.at[7])
+    out_v = pltpu.make_async_copy(qkv.at[2], v_out, loc.at[8])
+    out_k.start()
+    out_v.start()
+    in_wo.wait()
+    each(n, att_wait)
+    full = jnp.dot(att[...], wov[...], preferred_element_type=F32).astype(BF)
+    oc = o_send.shape[2]
+    for t in range(nt):
+        o_send[t] = full[:, t * oc : (t + 1) * oc]
+
+    def o_copy(d):
+        return to_tp(0, d, o_send.at[lax.rem(mt + d, nt)], o_recv.at[d])
+
+    def sq2_copy(d):
+        return to_tp(1, d, sq2_send, sq2_recv.at[d])
+
+    each(nt, lambda d: o_copy(d).start())
+    mixed = o_send[mt].astype(F32)
+    for d in range(1, nt):
+        o_copy(d).wait_recv()
+        mixed = mixed + o_recv[d].astype(F32)
+    sq_send[...] = dot_hi(jnp.ones((8, oc), F32), mixed * mixed, NT)
+    each(n, lambda d: sq_copy(d).start())
+    sq = sq_send[...]
+    for d in range(1, n):
+        sq_copy(d).wait_recv()
+        sq = sq + sq_recv[d]
+    sq2_send[...] = sq
+    each(nt, lambda d: sq2_copy(d).start())
+    for d in range(1, nt):
+        sq2_copy(d).wait_recv()
+        sq = sq + sq2_recv[d]
+    ssum = dot_hi(sq, jnp.full((8, oc), 0.125, F32), (((0,), (0,)), ((), ())))
+    mixed_out[...] = (mixed * lax.rsqrt(ssum / width + epsilon) * gpost[...]).astype(BF)
+
+    def drain(d):
+        for ph in range(3):
+            rs_copy(ph, d).wait_send()
+            ag_copy(ph, d).wait_send()
+        stat_copy(d).wait_send()
+        val_copy(d).wait_send()
+        cand_copy(d).wait_send()
+        att_copy(d).wait_send()
+        sq_copy(d).wait_send()
+
+    each(n, drain)
+
+    def drain_t(d):
+        o_copy(d).wait_send()
+        sq2_copy(d).wait_send()
+
+    each(nt, drain_t)
+    out_k.wait()
+    out_v.wait()
+
+
+def write_kernel(num_seqs, prop, heads, hd, span, kc, vc, kn, vn, lens, accs, k_out, v_out, buf, sin, sout):
+    base = lax.axis_index("kv") * span
+    hp = heads * prop
+    cols = heads * span
+    win = hp + 16
+    srcs, dsts, news = (kc, vc), (k_out, v_out), (kn, vn)
+    for s in range(num_seqs):
+        for i in range(2):
+            pltpu.make_async_copy(srcs[i].at[s], buf.at[i, s], sin.at[i, s]).start()
+    m = iota((win, hp), 1)
+    diff = iota((win, hp), 0) - (m % prop * heads + m // prop)
+    edge = iota((win, hd), 0)
+    for s in range(num_seqs):
+        first = (lens[s] + accs[s] - base) * heads
+        start = pl.multiple_of(jnp.clip(first // 16 * 16, 0, cols - win), 16)
+        sel = hot(diff == first - start).astype(BF)
+        here = edge - (first - start)
+        inside = (here >= 0) & (here < hp)
+        for i in range(2):
+            new = news[i][s * prop : (s + 1) * prop, :]
+            new = jnp.concatenate([new[:, h * hd : (h + 1) * hd] for h in range(heads)], axis=0)
+            placed = jnp.dot(sel, new, preferred_element_type=F32)
+            pltpu.make_async_copy(srcs[i].at[s], buf.at[i, s], sin.at[i, s]).wait()
+            old = buf[i, s, pl.ds(start, win), :].astype(F32)
+            buf[i, s, pl.ds(start, win), :] = jnp.where(inside, placed, old).astype(BF)
+            pltpu.make_async_copy(buf.at[i, s], dsts[i].at[s], sout.at[i, s]).start()
+    for s in range(num_seqs):
+        for i in range(2):
+            pltpu.make_async_copy(buf.at[i, s], dsts[i].at[s], sout.at[i, s]).wait()
+
+
+def fast_device(
+    n,
+    nt,
+    tokens,
+    gain_pre,
+    w_query,
+    w_key,
+    w_value,
+    w_forget,
+    b_forget,
+    w_out,
+    gain_post,
+    key_cache,
+    value_cache,
+    cum_cache,
+    lengths,
+    accepted,
+    parent,
+):
+    num_seqs, prop, width = tokens.shape
+    span, heads, hd = key_cache.shape[1:]
+    rows = num_seqs * prop
+    hw = heads * hd
+    cols = heads * span
+    sp = num_seqs // n
+    R = sp * prop
+    L = sp * heads * prop
+    oc = gain_post.shape[0]
+    kc = key_cache.reshape(num_seqs, cols, hd)
+    vc = value_cache.reshape(num_seqs, cols, hd)
+    cum = jnp.swapaxes(cum_cache, 1, 2).reshape(num_seqs * heads, span)
+    anyspec = pl.BlockSpec(memory_space=pl.ANY)
+    vmem = pl.BlockSpec(memory_space=pltpu.VMEM)
+    smem = pl.BlockSpec(memory_space=pltpu.SMEM)
+    V = pltpu.VMEM
+    D = pltpu.SemaphoreType.DMA
+    mixed, k_new, v_new, cum_new = pl.pallas_call(
+        functools.partial(layer_kernel, n, nt, num_seqs, prop, heads, hd, span),
+        out_shape=(
+            jax.ShapeDtypeStruct((rows, oc), BF),
+            jax.ShapeDtypeStruct((rows, hw), BF),
+            jax.ShapeDtypeStruct((rows, hw), BF),
+            jax.ShapeDtypeStruct(cum.shape, F32),
+        ),
+        in_specs=[
+            anyspec,
+            vmem,
+            anyspec,
+            anyspec,
+            anyspec,
+            vmem,
+            smem,
+            anyspec,
+            vmem,
+            anyspec,
+            anyspec,
+            vmem,
+            smem,
+            smem,
+            vmem,
+        ],
+        out_specs=(vmem, anyspec, anyspec, vmem),
+        scratch_shapes=[
+            V((rows, width), BF),
+            V((rows, width), BF),
+            V((3,) + w_query.shape, BF),
+            V(w_out.shape, BF),
+            V(kc.shape, BF),
+            V(vc.shape, BF),
+            V((3, rows, hw), BF),
+            V((3, n, R, hw), BF),
+            V((3, rows, hw), BF),
+            V((n, 8, L), F32),
+            V((n, L, hd), BF),
+            V((n, 8, L), F32),
+            V((n, L, hd), BF),
+            V((8, 128), F32),
+            V((n, 8, 128), F32),
+            V((num_seqs, cols), F32),
+            V((rows, rows), F32),
+            V((num_seqs, 128), F32),
+            V((num_seqs * heads, 128), F32),
+            V((rows, hw), BF),
+            V((nt, rows, oc), BF),
+            V((nt, rows, oc), BF),
+            V((8, rows), F32),
+            V((n, 8, rows), F32),
+            V((8, rows), F32),
+            V((nt, 8, rows), F32),
+            D((9,)),
+            D((11, n)),
+            D((11, n)),
+            D((2, nt)),
+            D((2, nt)),
+        ],
+        compiler_params=pltpu.CompilerParams(
+            collective_id=0, has_side_effects=True, vmem_limit_bytes=50 * 1024 * 1024
+        ),
+        name="layer",
+    )(
+        tokens.reshape(rows, width),
+        gain_pre.reshape(1, width),
+        w_query,
+        w_key,
+        w_value,
+        w_forget.T,
+        b_forget,
+        w_out,
+        gain_post.reshape(1, oc),
+        kc,
+        vc,
+        cum,
+        lengths,
+        accepted,
+        parent,
+    )
+    key_out, value_out = pl.pallas_call(
+        functools.partial(write_kernel, num_seqs, prop, heads, hd, span),
+        out_shape=(
+            jax.ShapeDtypeStruct(kc.shape, BF),
+            jax.ShapeDtypeStruct(vc.shape, BF),
+        ),
+        in_specs=[anyspec, anyspec, vmem, vmem, smem, smem],
+        out_specs=(anyspec, anyspec),
+        scratch_shapes=[
+            V((2,) + kc.shape, BF),
+            D((2, num_seqs)),
+            D((2, num_seqs)),
+        ],
+        compiler_params=pltpu.CompilerParams(vmem_limit_bytes=16 * 1024 * 1024),
+        name="cache_write",
+    )(kc, vc, k_new, v_new, lengths, accepted)
+    cum_out = jnp.swapaxes(cum_new.reshape(num_seqs, heads, span), 1, 2)
+    return (
+        mixed.reshape(num_seqs, prop, oc),
+        key_out.reshape(key_cache.shape),
+        value_out.reshape(value_cache.shape),
+        cum_out,
+    )
+
+
+def choose(mesh):
+    n, nt = mesh.shape["kv"], mesh.shape["tp"]
+
+    def body(*args):
+        tokens, key_cache = args[0], args[9]
+        num_seqs, prop = tokens.shape[:2]
+        span, heads = key_cache.shape[1:3]
+        fits = (
+            num_seqs % n == 0
+            and (num_seqs // n) * heads * prop == 128
+            and span == 128
+            and num_seqs * heads <= 128
+            and prop % 16 == 0
+        )
+        if fits:
+            return fast_device(n, nt, *args)
+        return per_device(*args)
+
+    return body
+
+
 def solution(mesh):
     return jax.shard_map(
-        per_device,
+        choose(mesh),
         mesh=mesh,
         in_specs=(
             P(),

time: 295 us -> 98.3 us (0.33)
  blocking collectives: 130 us -> 0 us
  waiting for transfers between devices: 87 us -> 0 us
  Pallas kernels: 0 us -> 86 us
  other arithmetic: 19.7 us -> 0 us
  matrix products: 16.7 us -> 0 us
  local copies, waits for them, and re-layouts: 25.7 us -> 11.1 us
  between operations: 14.2 us -> 0.69 us
    all_gather x3 -> x0, blocking collectives: 90.6 us -> none  [merged(): gathered = jax.tree.map(lambda a: lax.all_gather(a, axis), part)]
    pallas_call x0 -> x2, Pallas kernels: none -> 86 us  [the longest x1 74.2 us: fast_device(): pl.pallas_call(functools.partial(layer_kernel, n, nt, num_seqs, prop, hea...]
    psum x1 -> x0, waiting for transfers between devices: 75.1 us -> none  [per_device(): lax.psum(key_part.astype(jnp.bfloat16), 'kv').astype(jnp.float32)]
    psum x1 -> x0, blocking collectives: 39.3 us -> none  [per_device(): squares = lax.psum(jnp.sum(mixed_sum * mixed_sum, axis=1), ('kv', 'tp'))]
    dot_general x17 -> x0, matrix products: 16.7 us -> none  [the longest x1 2.98 us: per_device(): jnp.einsum('bihd,bkhd->bihk', query, key_cache, preferred_element_type=jn...]
    unnamed x4 -> x0, waiting for transfers between devices: 11.8 us -> none
    dynamic_slice x12 -> x0, local copies, waits for them, and re-layouts: 8.72 us -> none  [the longest x11 8.64 us: take(): lax.dynamic_index_in_dim(a, source, 0, False)]
    add x17 -> x0, other arithmetic: 7.14 us -> none  [the longest x7 6.66 us: combine_parts(): first[2] * first_scale[..., None] + second[2] * second_scale[..., None]]
  transfers between devices with their start and end apart: 3 -> 0, of which waited for: 2 -> 0; matrix products, arithmetic and copies ran while one was open for 7% -> 0% of each run, Pallas kernels for 0% -> 0%
where the time goes in v1:
time: 98.3 us; the launch traced here: 97.8 us
  Pallas kernels  86 us (87%)
  local copies, waits for them, and re-layouts  11.1 us (11%)
    pallas_call x1, Pallas kernels, fast_device(): pl.pallas_call(functools.partial(layer_kernel, n, nt, num_seqs, prop, hea...  74.2 us
    pallas_call x1, Pallas kernels, fast_device(): pl.pallas_call(functools.partial(write_kernel, num_seqs, prop, heads, hd,...  11.8 us
    unnamed x30, local copies, waits for them, and re-layouts  11.1 us

profile of v1, /device:TPU:0, one launch (start us, length us, event | category | flops | bytes accessed | tf_op | source)
XLA Modules:
  0.0 97.8 jit_solution(13078138955926832517)
XLA Ops:
  0.6 0.0 copy-start.2
  0.6 1.0 %copy-done.2 = bf16[512,512]{1,0:T(8,128)(2,1)S(1)} copy-done((bf16[512,512]{1,0:T(8,128)(2,1)S(1)}, bf16[512,512]{1,0:T(8,128)(2,1)}, u32[]{:S(2)}) %copy-start.2) | copy-done | bytes 524312
  1.7 0.0 copy-start.3
  1.7 1.0 %copy-done.3 = bf16[512,512]{1,0:T(8,128)(2,1)S(1)} copy-done((bf16[512,512]{1,0:T(8,128)(2,1)S(1)}, bf16[512,512]{1,0:T(8,128)(2,1)}, u32[]{:S(2)}) %copy-start.3) | copy-done | bytes 524312
  2.7 0.0 copy-start.4
  2.7 1.0 %copy-done.4 = bf16[512,512]{1,0:T(8,128)(2,1)S(1)} copy-done((bf16[512,512]{1,0:T(8,128)(2,1)S(1)}, bf16[512,512]{1,0:T(8,128)(2,1)}, u32[]{:S(2)}) %copy-start.4) | copy-done | bytes 524312
  3.8 0.0 copy-start.5
  3.8 1.0 %copy-done.5 = bf16[512,512]{1,0:T(8,128)(2,1)S(1)} copy-done((bf16[512,512]{1,0:T(8,128)(2,1)S(1)}, bf16[512,512]{1,0:T(8,128)(2,1)}, u32[]{:S(2)}) %copy-start.5) | copy-done | bytes 524312
  4.8 0.0 copy-start.6
  4.8 0.9 copy-done.6
  5.7 0.0 copy-start.7
  5.7 0.8 copy-done.7
  6.5 0.7 copy-done.8
  7.2 0.7 copy-done.9
  7.9 0.7 copy-done.10
  8.5 0.7 copy-done.11
  9.2 0.7 copy-done.12
  9.9 0.7 copy-done.13
  10.5 74.2 %layer.1 = (bf16[256,128]{1,0:T(8,128)(2,1)S(1)}, bf16[256,512]{1,0:T(8,128)(2,1)S(1)}, bf16[256,512]{1,0:T(8,128)(2,1)S(1)}, f32[64,128]{1,0:T(8,128)S(1)}) custom-call(bf16[256,4096]{1,0:T(8,128)(2,1)} %bitcast.25, f32[1,4096]{1,0:T(1,128)S(1)} %bitcast.23, bf16[512,512]{1,0:T(8,128)(2,1)S(1)} %copy-done.2, bf16[512,512]{1,0:T(8,128)(2,1)S(1)} %copy-done.3, ...), custom_call_target="tpu_custom_call" | custom-call | tf_op jit(solution)/shard_map/layer/pallas_call | solution.py:711
  84.7 0.0 copy-done
  84.7 0.0 copy-done.1
  84.7 11.8 %cache_write.1 = (bf16[16,512,128]{2,1,0:T(8,128)(2,1)}, bf16[16,512,128]{2,1,0:T(8,128)(2,1)}) custom-call(bf16[16,512,128]{2,1,0:T(8,128)(2,1)S(1)} %bitcast.16, bf16[16,512,128]{2,1,0:T(8,128)(2,1)S(1)} %bitcast.18, bf16[256,512]{1,0:T(8,128)(2,1)S(1)} %get-tuple-element.11.kn, bf16[256,512]{1,0:T(8,128)(2,1)S(1)} %get-tuple-element.12.vn, ...), custom_call_target="tpu_custom_call" | custom-call | tf_op jit(solution)/shard_map/cache_write/pallas_call | solution.py:791
  96.5 0.6 copy.21
  97.1 0.6 copy.22
  (8 shorter events, 0.0 us)
Async XLA Ops:
  0.6 1.0 %copy-start.2 = (bf16[512,512]{1,0:T(8,128)(2,1)S(1)}, bf16[512,512]{1,0:T(8,128)(2,1)}, u32[]{:S(2)}) copy-start(bf16[512,512]{1,0:T(8,128)(2,1)} %wq.1) | copy-start | bytes 1572868
  1.7 1.0 %copy-start.3 = (bf16[512,512]{1,0:T(8,128)(2,1)S(1)}, bf16[512,512]{1,0:T(8,128)(2,1)}, u32[]{:S(2)}) copy-start(bf16[512,512]{1,0:T(8,128)(2,1)} %wk.1) | copy-start | bytes 1572868
  2.7 1.0 %copy-start.4 = (bf16[512,512]{1,0:T(8,128)(2,1)S(1)}, bf16[512,512]{1,0:T(8,128)(2,1)}, u32[]{:S(2)}) copy-start(bf16[512,512]{1,0:T(8,128)(2,1)} %wv.1) | copy-start | bytes 1572868
  3.8 1.0 %copy-start.5 = (bf16[512,512]{1,0:T(8,128)(2,1)S(1)}, bf16[512,512]{1,0:T(8,128)(2,1)}, u32[]{:S(2)}) copy-start(bf16[512,512]{1,0:T(8,128)(2,1)} %wo.1) | copy-start | bytes 1572868
  4.8 0.9 copy-start.6
  5.7 0.8 copy-start.7
  6.5 0.7 copy-start.8
  7.2 0.7 copy-start.9
  7.9 0.7 copy-start.10
  8.5 0.7 copy-start.11
  9.2 0.7 copy-start.12
  9.9 0.7 copy-start.13
  10.5 74.2 %copy-start = (bf16[16,128,4,128]{3,2,1,0:T(4,128)(2,1)S(1)}, bf16[16,128,4,128]{3,2,1,0:T(4,128)(2,1)}, u32[]{:S(2)}) copy-start(bf16[16,128,4,128]{3,2,1,0:T(4,128)(2,1)} %param.24) | copy-start | bytes 6291460
  10.5 74.2 %copy-start.1 = (bf16[16,128,4,128]{3,2,1,0:T(4,128)(2,1)S(1)}, bf16[16,128,4,128]{3,2,1,0:T(4,128)(2,1)}, u32[]{:S(2)}) copy-start(bf16[16,128,4,128]{3,2,1,0:T(4,128)(2,1)} %param.25) | copy-start | bytes 6291460

commit v2 on v1

--- a/solution.py
+++ b/solution.py
@@ -224,33 +224,47 @@
     hd,
     span,
     tok,
-    gain,
+    gain_h,
     wq,
     wk,
     wv,
-    wft,
-    bias,
+    wft_h,
+    bias_h,
     wo,
-    gpost,
+    gpost_h,
     kc,
     vc,
-    cum,
-    lens,
-    accs,
-    parent,
+    cum_h,
+    lens_h,
+    accs_h,
+    parent_h,
     mixed_out,
-    k_out,
-    v_out,
+    kv_out,
     cum_out,
     tokv,
     normed,
+    gain,
     wv3,
+    wft,
     wov,
+    gpost,
     kcv,
     vcv,
-    part,
-    rs_recv,
-    qkv,
+    cum,
+    parent,
+    bias,
+    lens,
+    accs,
+    partq,
+    rsq,
+    part2,
+    rs1,
+    half,
+    rs2,
+    kvown,
+    flat,
+    kvflat,
+    qall,
     st_send,
     val_send,
     st_recv,
@@ -306,17 +320,29 @@
     lax.fori_loop(1, n, greet, 0)
     lax.fori_loop(1, nt, greet_t, 0)
 
-    in_tok = pltpu.make_async_copy(tok, tokv, loc.at[0])
-    in_w = [pltpu.make_async_copy(w, wv3.at[i], loc.at[1 + i]) for i, w in enumerate((wq, wk, wv))]
-    in_kc = pltpu.make_async_copy(kc, kcv, loc.at[4])
-    in_vc = pltpu.make_async_copy(vc, vcv, loc.at[5])
-    in_wo = pltpu.make_async_copy(wo, wov, loc.at[6])
-    in_tok.start()
-    for c in in_w:
+    pairs = (
+        (tok, tokv),
+        (gain_h, gain),
+        (wq, wv3.at[0]),
+        (wk, wv3.at[1]),
+        (wv, wv3.at[2]),
+        (cum_h, cum),
+        (lens_h, lens),
+        (accs_h, accs),
+        (parent_h, parent),
+        (bias_h, bias),
+        (wft_h, wft),
+        (kc, kcv),
+        (vc, vcv),
+        (wo, wov),
+        (gpost_h, gpost),
+    )
+    ins = [pltpu.make_async_copy(a, b, loc.at[i]) for i, (a, b) in enumerate(pairs)]
+    for c in ins:
         c.start()
-    in_kc.start()
-    in_vc.start()
-    in_wo.start()
+    par = lax.rem(me, 2)
+    mate = me + 1 - 2 * par
+    nh = n // 2
 
     def to_kv(ph, d, src, dst, sign=1):
         peer = lax.rem(me + sign * d + n, n)
@@ -349,14 +375,68 @@
     def rrow(i):
         return pl.ds(pl.multiple_of(i * R, R), R)
 
-    def rs_copy(ph, d):
-        return to_kv(ph, d, part.at[ph, rrow(up(d))], rs_recv.at[ph, d])
-
-    def ag_copy(ph, d):
-        return to_kv(3 + ph, d, qkv.at[ph, rrow(me)], qkv.at[ph, rrow(me)])
-
-    def ag_wait(ph, d):
-        to_kv(3 + ph, d, qkv.at[ph, rrow(me)], qkv.at[ph, rrow(down(d))]).wait_recv()
+    def lrow(i):
+        return pl.ds(pl.multiple_of(i * L, L), L)
+
+    def to_peer(ph, d, peer, src, dst):
+        return pltpu.make_async_remote_copy(
+            src_ref=src,
+            dst_ref=dst,
+            send_sem=ssem.at[ph, d],
+            recv_sem=rsem.at[ph, d],
+            device_id={"kv": peer},
+            device_id_type=MESH,
+        )
+
+    def rsq_copy(d):
+        return to_kv(0, d, partq.at[rrow(up(d))], rsq.at[d])
+
+    def rs1_copy():
+        return to_peer(1, 0, mate, part2.at[1 - par], rs1)
+
+    def rs2_copy(e):
+        peer = up(2 * e)
+        return to_peer(2, e, peer, half.at[peer // 2], rs2.at[e])
+
+    def gather_along(ph, e, view):
+        return to_peer(ph, 2 * e, up(2 * e), view(me), view(me))
+
+    def gather_mate(ph, e, view):
+        c = down(2 * e)
+        return to_peer(ph, 2 * e + 1, mate, view(c), view(c))
+
+    def gather_start(ph, view):
+        each(nh, lambda e: gather_along(ph, e, view).start())
+        gather_mate(ph, 0, view).start()
+
+    def gather_pass(ph, view):
+        def one(e):
+            c = down(2 * e)
+            to_peer(ph, 2 * e, me, view(c), view(c)).wait_recv()
+            gather_mate(ph, e, view).start()
+
+        each(nh, one)
+
+    def mate_chunk(e):
+        return lax.rem(mate - 2 * e + n, n)
+
+    def gather_wait(ph, e, view):
+        c = mate_chunk(e)
+        to_peer(ph, 2 * e + 1, mate, view(c), view(c)).wait_recv()
+
+    def gather_drain(ph, view):
+        each(nh, lambda e: gather_along(ph, e, view).wait_send())
+        for e in range(nh):
+            gather_mate(ph, e, view).wait_send()
+
+    def q_view(c):
+        return qall.at[rrow(c)]
+
+    def kv_view(c):
+        return kvflat.at[:, lrow(c)]
+
+    def att_view(c):
+        return att.at[rrow(c)]
 
     def stat_copy(d):
         return to_kv(6, d, st_send.at[d], st_recv.at[d], -1)
@@ -366,12 +446,6 @@
 
     def cand_copy(d):
         return to_kv(8, d, cand_send, cand_recv.at[d])
-
-    def att_copy(d):
-        return to_kv(9, d, att.at[rrow(me)], att.at[rrow(me)])
-
-    def att_wait(d):
-        to_kv(9, d, att.at[rrow(me)], att.at[rrow(down(d))]).wait_recv()
 
     def sq_copy(d):
         return to_kv(10, d, sq_send, sq_recv.at[d])
@@ -383,7 +457,8 @@
 
         lax.fori_loop(1, count, body, 0)
 
-    in_tok.wait()
+    ins[0].wait()
+    ins[1].wait()
     nb = prop
 
     def norm_rows(i, c):
@@ -396,10 +471,16 @@
     lax.fori_loop(0, rows // nb, norm_rows, 0)
     local = normed[:, pl.ds(pl.multiple_of(me * kdim, kdim), kdim)]
     pl.semaphore_wait(barrier, n - 1 + nt - 1)
-    for ph in range(3):
-        in_w[ph].wait()
-        part[ph] = jnp.dot(local, wv3[ph], preferred_element_type=F32).astype(BF)
-        each(n, lambda d: rs_copy(ph, d).start())
+    ins[2].wait()
+    partq[...] = jnp.dot(local, wv3[0], preferred_element_type=F32).astype(BF)
+    each(n, lambda d: rsq_copy(d).start())
+    for i in range(2):
+        ins[3 + i].wait()
+        both_rows = jnp.dot(local, wv3[1 + i], preferred_element_type=F32).astype(BF)
+        for c in range(n):
+            part2[c % 2, c // 2, :, i * hw : (i + 1) * hw] = both_rows[c * R : (c + 1) * R]
+    for c in ins[5:11]:
+        c.wait()
 
     r64 = num_seqs * heads
     c64 = cum[...]
@@ -456,31 +537,27 @@
     ptm = jnp.where((iota((r64, 128), 1) // prop) % heads == iota((r64, 128), 0) % heads, pt, 0.0)
     tpath[...] = dot_hi(take, ptm)
 
-    def reduce_part(ph):
-        total = part[ph, rrow(me)].astype(F32)
-        for d in range(1, n):
-            rs_copy(ph, d).wait_recv()
-            total = total + rs_recv[ph, d].astype(F32)
-        qkv[ph, rrow(me)] = total.astype(BF)
-        each(n, lambda d: ag_copy(ph, d).start())
-
-    for ph in range(3):
-        reduce_part(ph)
-
-    in_kc.wait()
-    in_vc.wait()
+    own_q = partq[rrow(me)].astype(F32)
+    for d in range(1, n):
+        rsq_copy(d).wait_recv()
+        own_q = own_q + rsq[d].astype(F32)
+    qall[rrow(me)] = own_q.astype(BF)
+    gather_start(3, q_view)
+    rs1_copy().start()
+
+    ins[11].wait()
+    ins[12].wait()
     same_head = iota((hp, cols), 0) // prop == iota((hp, cols), 1) % heads
     diag_l = iota((L, L), 0) == iota((L, L), 1)
 
-    def heads_of(ph, s):
-        block = qkv[ph, pl.ds(pl.multiple_of(s * prop, prop), prop), :]
+    def heads_of(block):
         return jnp.concatenate([block[:, h * hd : (h + 1) * hd] for h in range(heads)], axis=0)
 
     def block_part(src):
         maxes, totals, values = [], [], []
         for j in range(sp):
             s = src * sp + j
-            q = heads_of(0, s)
+            q = heads_of(qall[pl.ds(pl.multiple_of(s * prop, prop), prop), :])
             sc = lax.dot_general(q, kcv[s], NT, preferred_element_type=F32) * scale
             sc = jnp.where(same_head, sc + brow[pl.ds(s, 1), :], floor_value)
             m = jnp.max(sc, axis=1, keepdims=True)
@@ -498,25 +575,46 @@
         return stats, jnp.concatenate(values, axis=0)
 
     def remote_block(d):
-        ag_wait(0, d)
-        stats, values = block_part(down(d))
+        src = down(d)
+        stats, values = block_part(src)
         st_send[d] = stats
         val_send[d] = values
         stat_copy(d).start()
         val_copy(d).start()
 
-    each(n, remote_block)
     stats, values = block_part(me)
     st_recv[0] = stats
     val_recv[0] = values
+    gather_pass(3, q_view)
+    each(nh, lambda e: remote_block(2 * e))
+    rs1_copy().wait_recv()
+    for i in range(nh):
+        half[i] = (part2[par, i].astype(F32) + rs1[i].astype(F32)).astype(BF)
+    each(nh, lambda e: rs2_copy(e).start())
+
+    def mate_block(e, c):
+        gather_wait(3, e, q_view)
+        remote_block(lax.rem(me - mate_chunk(e) + n, n))
+        return c
+
+    lax.fori_loop(0, nh, mate_block, 0)
+    own_kv = half[me // 2].astype(F32)
+    for e in range(1, nh):
+        rs2_copy(e).wait_recv()
+        own_kv = own_kv + rs2[e].astype(F32)
+    kvown[...] = own_kv.astype(BF)
+    for i in range(2):
+        for h in range(heads):
+            flat[pl.ds(h, R, stride=heads), :] = own_kv[:, i * hw + h * hd : i * hw + (h + 1) * hd]
+        kvflat[i, lrow(me)] = flat[...].astype(BF)
 
     fold_h = iota((rows, hp), 0)
     tmax, ttot, tval = [], [], []
     for j in range(sp):
         s = me * sp + j
-        q = heads_of(0, s)
-        k = heads_of(1, s)
-        v = heads_of(2, s)
+        q = heads_of(qall[pl.ds(pl.multiple_of(s * prop, prop), prop), :])
+        k = heads_of(kvown[j * prop : (j + 1) * prop, 0:hw])
+        v = heads_of(kvown[j * prop : (j + 1) * prop, hw : 2 * hw])
         arows = anc[pl.ds(pl.multiple_of(s * prop, prop), prop), :]
         sel = hot(fold_h == s * prop + iota((rows, hp), 1) % prop).astype(BF)
         am = jnp.dot(arows.astype(BF), sel, preferred_element_type=F32)
@@ -581,15 +679,13 @@
             att[pl.ds(pl.multiple_of(me * R + j * prop, prop), prop), h * hd : (h + 1) * hd] = (
                 attended[j * hp + h * prop : j * hp + (h + 1) * prop]
             )
-    each(n, lambda d: att_copy(d).start())
-    each(n, lambda d: ag_wait(1, d))
-    each(n, lambda d: ag_wait(2, d))
-    out_k = pltpu.make_async_copy(qkv.at[1], k_out, loc.at[7])
-    out_v = pltpu.make_async_copy(qkv.at[2], v_out, loc.at[8])
-    out_k.start()
-    out_v.start()
-    in_wo.wait()
-    each(n, att_wait)
+    gather_start(4, att_view)
+    gather_start(5, kv_view)
+    ins[13].wait()
+    ins[14].wait()
+    gather_pass(4, att_view)
+    for e in range(nh):
+        gather_wait(4, e, att_view)
     full = jnp.dot(att[...], wov[...], preferred_element_type=F32).astype(BF)
     oc = o_send.shape[2]
     for t in range(nt):
@@ -602,12 +698,17 @@
         return to_tp(1, d, sq2_send, sq2_recv.at[d])
 
     each(nt, lambda d: o_copy(d).start())
+    gather_pass(5, kv_view)
     mixed = o_send[mt].astype(F32)
     for d in range(1, nt):
         o_copy(d).wait_recv()
         mixed = mixed + o_recv[d].astype(F32)
     sq_send[...] = dot_hi(jnp.ones((8, oc), F32), mixed * mixed, NT)
     each(n, lambda d: sq_copy(d).start())
+    for e in range(nh):
+        gather_wait(5, e, kv_view)
+    out_kv = pltpu.make_async_copy(kvflat, kv_out, loc.at[15])
+    out_kv.start()
     sq = sq_send[...]
     for d in range(1, n):
         sq_copy(d).wait_recv()
@@ -621,55 +722,109 @@
     mixed_out[...] = (mixed * lax.rsqrt(ssum / width + epsilon) * gpost[...]).astype(BF)
 
     def drain(d):
-        for ph in range(3):
-            rs_copy(ph, d).wait_send()
-            ag_copy(ph, d).wait_send()
+        rsq_copy(d).wait_send()
         stat_copy(d).wait_send()
         val_copy(d).wait_send()
         cand_copy(d).wait_send()
-        att_copy(d).wait_send()
         sq_copy(d).wait_send()
 
     each(n, drain)
+    rs1_copy().wait_send()
+    each(nh, lambda e: rs2_copy(e).wait_send())
+    gather_drain(3, q_view)
+    gather_drain(4, att_view)
+    gather_drain(5, kv_view)
 
     def drain_t(d):
         o_copy(d).wait_send()
         sq2_copy(d).wait_send()
 
     each(nt, drain_t)
-    out_k.wait()
-    out_v.wait()
-
-
-def write_kernel(num_seqs, prop, heads, hd, span, kc, vc, kn, vn, lens, accs, k_out, v_out, buf, sin, sout):
+    out_kv.wait()
+
+
+def write_kernel(
+    num_seqs,
+    prop,
+    span,
+    kc,
+    vc,
+    kv_new,
+    mixed,
+    cum,
+    lens_h,
+    accs_h,
+    k_out,
+    v_out,
+    mixed_out,
+    cum_out,
+    buf,
+    fresh,
+    lens,
+    accs,
+    sem,
+    sin,
+    sout,
+):
     base = lax.axis_index("kv") * span
-    hp = heads * prop
-    cols = heads * span
-    win = hp + 16
-    srcs, dsts, news = (kc, vc), (k_out, v_out), (kn, vn)
-    for s in range(num_seqs):
+    small = [
+        pltpu.make_async_copy(lens_h, lens, sem.at[0]),
+        pltpu.make_async_copy(accs_h, accs, sem.at[1]),
+        pltpu.make_async_copy(kv_new, fresh, sem.at[2]),
+        pltpu.make_async_copy(mixed, mixed_out, sem.at[3]),
+        pltpu.make_async_copy(cum, cum_out, sem.at[4]),
+    ]
+    cut = sin.shape[1]
+    step = num_seqs // cut
+    arrays = ((kc, k_out), (vc, v_out))
+
+    def part(c):
+        return pl.ds(c * step, step)
+
+    def come(c, i):
+        return pltpu.make_async_copy(arrays[i][0].at[part(c)], buf.at[i, part(c)], sin.at[i, c])
+
+    def leave(c, i):
+        return pltpu.make_async_copy(buf.at[i, part(c)], arrays[i][1].at[part(c)], sout.at[i, c])
+
+    for c in small[:3]:
+        c.start()
+    for c in range(cut):
         for i in range(2):
-            pltpu.make_async_copy(srcs[i].at[s], buf.at[i, s], sin.at[i, s]).start()
-    m = iota((win, hp), 1)
-    diff = iota((win, hp), 0) - (m % prop * heads + m // prop)
-    edge = iota((win, hd), 0)
-    for s in range(num_seqs):
-        first = (lens[s] + accs[s] - base) * heads
-        start = pl.multiple_of(jnp.clip(first // 16 * 16, 0, cols - win), 16)
-        sel = hot(diff == first - start).astype(BF)
-        here = edge - (first - start)
-        inside = (here >= 0) & (here < hp)
+            come(c, i).start()
+    for c in small[3:]:
+        c.start()
+    for c in small[:3]:
+        c.wait()
+
+    def place(i, s):
+        rel = lens[s] + accs[s] - base
+        whole = (rel >= 0) & (rel <= span - prop)
+        partly = (rel > -prop) & (rel < span) & jnp.logical_not(whole)
+
+        @pl.when(whole)
+        def _():
+            buf[i, s, pl.ds(rel, prop)] = fresh[i, s]
+
+        @pl.when(partly)
+        def _():
+            def one(j, c):
+                buf[i, s, pl.ds(rel + j, 1)] = fresh[i, s, pl.ds(j, 1)]
+                return c
+
+            lax.fori_loop(jnp.maximum(-rel, 0), jnp.minimum(span - rel, prop), one, 0)
+
+    for c in range(cut):
         for i in range(2):
-            new = news[i][s * prop : (s + 1) * prop, :]
-            new = jnp.concatenate([new[:, h * hd : (h + 1) * hd] for h in range(heads)], axis=0)
-            placed = jnp.dot(sel, new, preferred_element_type=F32)
-            pltpu.make_async_copy(srcs[i].at[s], buf.at[i, s], sin.at[i, s]).wait()
-            old = buf[i, s, pl.ds(start, win), :].astype(F32)
-            buf[i, s, pl.ds(start, win), :] = jnp.where(inside, placed, old).astype(BF)
-            pltpu.make_async_copy(buf.at[i, s], dsts[i].at[s], sout.at[i, s]).start()
-    for s in range(num_seqs):
+            come(c, i).wait()
+            for s in range(c * step, (c + 1) * step):
+                place(i, s)
+            leave(c, i).start()
+    for c in range(cut):
         for i in range(2):
-            pltpu.make_async_copy(buf.at[i, s], dsts[i].at[s], sout.at[i, s]).wait()
+            leave(c, i).wait()
+    for c in small[3:]:
+        c.wait()
 
 
 def fast_device(
@@ -703,47 +858,46 @@
     kc = key_cache.reshape(num_seqs, cols, hd)
     vc = value_cache.reshape(num_seqs, cols, hd)
     cum = jnp.swapaxes(cum_cache, 1, 2).reshape(num_seqs * heads, span)
-    anyspec = pl.BlockSpec(memory_space=pl.ANY)
     vmem = pl.BlockSpec(memory_space=pltpu.VMEM)
-    smem = pl.BlockSpec(memory_space=pltpu.SMEM)
     V = pltpu.VMEM
     D = pltpu.SemaphoreType.DMA
-    mixed, k_new, v_new, cum_new = pl.pallas_call(
+    hbm = pl.BlockSpec(memory_space=pltpu.HBM)
+    S = pltpu.SMEM
+    nh = n // 2
+    mixed, kv_new, cum_new = pl.pallas_call(
         functools.partial(layer_kernel, n, nt, num_seqs, prop, heads, hd, span),
         out_shape=(
             jax.ShapeDtypeStruct((rows, oc), BF),
-            jax.ShapeDtypeStruct((rows, hw), BF),
-            jax.ShapeDtypeStruct((rows, hw), BF),
+            jax.ShapeDtypeStruct((2, rows * heads, hd), BF),
             jax.ShapeDtypeStruct(cum.shape, F32),
         ),
-        in_specs=[
-            anyspec,
-            vmem,
-            anyspec,
-            anyspec,
-            anyspec,
-            vmem,
-            smem,
-            anyspec,
-            vmem,
-            anyspec,
-            anyspec,
-            vmem,
-            smem,
-            smem,
-            vmem,
-        ],
-        out_specs=(vmem, anyspec, anyspec, vmem),
+        in_specs=[hbm] * 15,
+        out_specs=(vmem, hbm, vmem),
         scratch_shapes=[
             V((rows, width), BF),
             V((rows, width), BF),
+            V((1, width), F32),
             V((3,) + w_query.shape, BF),
+            V(w_forget.T.shape, BF),
             V(w_out.shape, BF),
+            V((1, oc), F32),
             V(kc.shape, BF),
             V(vc.shape, BF),
-            V((3, rows, hw), BF),
-            V((3, n, R, hw), BF),
-            V((3, rows, hw), BF),
+            V(cum.shape, F32),
+            V(parent.shape, jnp.int32),
+            S(b_forget.shape, F32),
+            S(lengths.shape, jnp.int32),
+            S(accepted.shape, jnp.int32),
+            V((rows, hw), BF),
+            V((n, R, hw), BF),
+            V((2, nh, R, 2 * hw), BF),
+            V((nh, R, 2 * hw), BF),
+            V((nh, R, 2 * hw), BF),
+            V((nh, R, 2 * hw), BF),
+            V((R, 2 * hw), BF),
+            V((L, hd), F32),
+            V((2, rows * heads, hd), BF),
+            V((rows, hw), BF),
             V((n, 8, L), F32),
             V((n, L, hd), BF),
             V((n, 8, L), F32),
@@ -761,14 +915,14 @@
             V((n, 8, rows), F32),
             V((8, rows), F32),
             V((nt, 8, rows), F32),
-            D((9,)),
+            D((16,)),
             D((11, n)),
             D((11, n)),
             D((2, nt)),
             D((2, nt)),
         ],
         compiler_params=pltpu.CompilerParams(
-            collective_id=0, has_side_effects=True, vmem_limit_bytes=50 * 1024 * 1024
+            collective_id=0, has_side_effects=True, vmem_limit_bytes=67043328
         ),
         name="layer",
     )(
@@ -788,27 +942,41 @@
         accepted,
         parent,
     )
-    key_out, value_out = pl.pallas_call(
-        functools.partial(write_kernel, num_seqs, prop, heads, hd, span),
+    key_out, value_out, mixed, cum_new = pl.pallas_call(
+        functools.partial(write_kernel, num_seqs, prop, span),
         out_shape=(
-            jax.ShapeDtypeStruct(kc.shape, BF),
-            jax.ShapeDtypeStruct(vc.shape, BF),
+            jax.ShapeDtypeStruct(key_cache.shape, BF),
+            jax.ShapeDtypeStruct(value_cache.shape, BF),
+            jax.ShapeDtypeStruct(mixed.shape, BF),
+            jax.ShapeDtypeStruct(cum_new.shape, F32),
         ),
-        in_specs=[anyspec, anyspec, vmem, vmem, smem, smem],
-        out_specs=(anyspec, anyspec),
+        in_specs=[hbm] * 7,
+        out_specs=(hbm,) * 4,
         scratch_shapes=[
-            V((2,) + kc.shape, BF),
-            D((2, num_seqs)),
-            D((2, num_seqs)),
+            V((2,) + key_cache.shape, BF),
+            V((2, num_seqs, prop, heads, hd), BF),
+            S(lengths.shape, jnp.int32),
+            S(accepted.shape, jnp.int32),
+            D((5,)),
+            D((2, 4)),
+            D((2, 4)),
         ],
-        compiler_params=pltpu.CompilerParams(vmem_limit_bytes=16 * 1024 * 1024),
+        compiler_params=pltpu.CompilerParams(vmem_limit_bytes=67043328),
         name="cache_write",
-    )(kc, vc, k_new, v_new, lengths, accepted)
+    )(
+        key_cache,
+        value_cache,
+        kv_new.reshape(2, num_seqs, prop, heads, hd),
+        mixed,
+        cum_new,
+        lengths,
+        accepted,
+    )
     cum_out = jnp.swapaxes(cum_new.reshape(num_seqs, heads, span), 1, 2)
     return (
         mixed.reshape(num_seqs, prop, oc),
-        key_out.reshape(key_cache.shape),
-        value_out.reshape(value_cache.shape),
+        key_out,
+        value_out,
         cum_out,
     )
 
@@ -822,6 +990,8 @@
         span, heads = key_cache.shape[1:3]
         fits = (
             num_seqs % n == 0
+            and n % 2 == 0
+            and num_seqs % 4 == 0
             and (num_seqs // n) * heads * prop == 128
             and span == 128
             and num_seqs * heads <= 128

time: 98.3 us -> 61.8 us (0.63)
  Pallas kernels: 86 us -> 61.1 us
  local copies, waits for them, and re-layouts: 11.1 us -> 0 us
    pallas_call x1, Pallas kernels: 74.2 us -> 56.7 us  [fast_device(): pl.pallas_call(functools.partial(layer_kernel, n, nt, num_seqs, prop, hea...]
    unnamed x30 -> x0, local copies, waits for them, and re-layouts: 11.1 us -> none
    pallas_call x1, Pallas kernels: 11.8 us -> 4.34 us  [fast_device(): pl.pallas_call(functools.partial(write_kernel, num_seqs, prop, span), out...]
where the time goes in v2:
time: 61.8 us; the launch traced here: 61.7 us
  Pallas kernels  61.1 us (99%)
  between operations  0.64 us (1%)
    pallas_call x1, Pallas kernels, fast_device(): pl.pallas_call(functools.partial(layer_kernel, n, nt, num_seqs, prop, hea...  56.7 us
    pallas_call x1, Pallas kernels, fast_device(): pl.pallas_call(functools.partial(write_kernel, num_seqs, prop, span), out...  4.34 us

profile of v2, /device:TPU:0, one launch (start us, length us, event | category | flops | bytes accessed | tf_op | source)
XLA Modules:
  0.0 61.7 jit_solution(5389214488085049609)
XLA Ops:
  0.6 56.7 %layer.1 = (bf16[256,128]{1,0:T(8,128)(2,1)}, bf16[2,1024,128]{2,1,0:T(8,128)(2,1)}, f32[64,128]{1,0:T(8,128)}) custom-call(bf16[256,4096]{1,0:T(8,128)(2,1)} %bitcast.16, f32[1,4096]{1,0:T(1,128)} %bitcast.20, bf16[512,512]{1,0:T(8,128)(2,1)} %wq.1, bf16[512,512]{1,0:T(8,128)(2,1)} %wk.1, bf16[512,512]{1,0:T(8,128)(2,1)} %wv.1, bf16[16,4096]{1,0:T(8,128)(2,1)} %bitcast.18, ...), custom_call_target="tpu_custom_call" | custom-call | tf_op jit(solution)/shard_map/layer/pallas_call | solution.py:867
  57.4 4.3 %cache_write.1 = (bf16[16,128,4,128]{3,2,1,0:T(4,128)(2,1)}, bf16[16,128,4,128]{3,2,1,0:T(4,128)(2,1)}, bf16[256,128]{1,0:T(8,128)(2,1)}, f32[64,128]{1,0:T(8,128)}) custom-call(bf16[16,128,4,128]{3,2,1,0:T(4,128)(2,1)} %kc.1, bf16[16,128,4,128]{3,2,1,0:T(4,128)(2,1)} %vc.1, bf16[2,16,16,4,128]{4,3,2,1,0:T(4,128)(2,1)} %bitcast.17, ...), custom_call_target="tpu_custom_call" | custom-call | tf_op jit(solution)/shard_map/cache_write/pallas_call | solution.py:945

commit v3 on v2

--- a/solution.py
+++ b/solution.py
@@ -243,6 +243,8 @@
     cum_out,
     tokv,
     normed,
+    slab,
+    invs,
     gain,
     wv3,
     wft,
@@ -338,7 +340,15 @@
         (gpost_h, gpost),
     )
     ins = [pltpu.make_async_copy(a, b, loc.at[i]) for i, (a, b) in enumerate(pairs)]
-    for c in ins:
+    pieces = 4
+    piece = rows // pieces
+    tok_in = [
+        pltpu.make_async_copy(
+            tok.at[pl.ds(i * piece, piece)], tokv.at[pl.ds(i * piece, piece)], loc.at[16 + i]
+        )
+        for i in range(pieces)
+    ]
+    for c in tok_in[:1] + ins[1:2] + tok_in[1:] + ins[2:5]:
         c.start()
     par = lax.rem(me, 2)
     mate = me + 1 - 2 * par
@@ -432,8 +442,11 @@
     def q_view(c):
         return qall.at[rrow(c)]
 
-    def kv_view(c):
-        return kvflat.at[:, lrow(c)]
+    def k_view(c):
+        return kvflat.at[0, lrow(c)]
+
+    def v_view(c):
+        return kvflat.at[1, lrow(c)]
 
     def att_view(c):
         return att.at[rrow(c)]
@@ -457,19 +470,24 @@
 
         lax.fori_loop(1, count, body, 0)
 
-    ins[0].wait()
+    nb = min(2 * prop, piece)
+    mine = pl.ds(pl.multiple_of(me * kdim, kdim), kdim)
     ins[1].wait()
-    nb = prop
 
     def norm_rows(i, c):
         sl = pl.ds(pl.multiple_of(i * nb, nb), nb)
         t = tokv[sl, :].astype(F32)
         inv = lax.rsqrt(jnp.mean(t * t, axis=-1, keepdims=True) + epsilon)
-        normed[sl, :] = (t * inv * gain[...]).astype(BF)
+        invs[sl, :] = jnp.broadcast_to(inv, (nb, 128))
+        slab[sl, :] = (tokv[sl, mine].astype(F32) * inv * gain[:, mine]).astype(BF)
         return c
 
-    lax.fori_loop(0, rows // nb, norm_rows, 0)
-    local = normed[:, pl.ds(pl.multiple_of(me * kdim, kdim), kdim)]
+    for p in range(pieces):
+        tok_in[p].wait()
+        lax.fori_loop(p * piece // nb, (p + 1) * piece // nb, norm_rows, 0)
+    for c in ins[5:]:
+        c.start()
+    local = slab[...]
     pl.semaphore_wait(barrier, n - 1 + nt - 1)
     ins[2].wait()
     partq[...] = jnp.dot(local, wv3[0], preferred_element_type=F32).astype(BF)
@@ -479,6 +497,13 @@
         both_rows = jnp.dot(local, wv3[1 + i], preferred_element_type=F32).astype(BF)
         for c in range(n):
             part2[c % 2, c // 2, :, i * hw : (i + 1) * hw] = both_rows[c * R : (c + 1) * R]
+    def norm_rest(i, c):
+        sl = pl.ds(pl.multiple_of(i * nb, nb), nb)
+        inv = invs[sl, 0:1]
+        normed[sl, :] = (tokv[sl, :].astype(F32) * inv * gain[...]).astype(BF)
+        return c
+
+    lax.fori_loop(0, rows // nb, norm_rest, 0)
     for c in ins[5:11]:
         c.wait()
 
@@ -607,6 +632,7 @@
         for h in range(heads):
             flat[pl.ds(h, R, stride=heads), :] = own_kv[:, i * hw + h * hd : i * hw + (h + 1) * hd]
         kvflat[i, lrow(me)] = flat[...].astype(BF)
+    gather_start(5, k_view)
 
     fold_h = iota((rows, hp), 0)
     tmax, ttot, tval = [], [], []
@@ -680,9 +706,10 @@
                 attended[j * hp + h * prop : j * hp + (h + 1) * prop]
             )
     gather_start(4, att_view)
-    gather_start(5, kv_view)
+    gather_start(11, v_view)
     ins[13].wait()
     ins[14].wait()
+    gather_pass(5, k_view)
     gather_pass(4, att_view)
     for e in range(nh):
         gather_wait(4, e, att_view)
@@ -698,27 +725,28 @@
         return to_tp(1, d, sq2_send, sq2_recv.at[d])
 
     each(nt, lambda d: o_copy(d).start())
-    gather_pass(5, kv_view)
+    gather_pass(11, v_view)
     mixed = o_send[mt].astype(F32)
     for d in range(1, nt):
         o_copy(d).wait_recv()
         mixed = mixed + o_recv[d].astype(F32)
-    sq_send[...] = dot_hi(jnp.ones((8, oc), F32), mixed * mixed, NT)
+    sq_send[...] = dot_hi(jnp.ones((8, oc), F32), mixed * mixed, NT)[0:1]
     each(n, lambda d: sq_copy(d).start())
-    for e in range(nh):
-        gather_wait(5, e, kv_view)
-    out_kv = pltpu.make_async_copy(kvflat, kv_out, loc.at[15])
-    out_kv.start()
     sq = sq_send[...]
     for d in range(1, n):
         sq_copy(d).wait_recv()
         sq = sq + sq_recv[d]
     sq2_send[...] = sq
     each(nt, lambda d: sq2_copy(d).start())
+    for e in range(nh):
+        gather_wait(5, e, k_view)
+        gather_wait(11, e, v_view)
+    out_kv = pltpu.make_async_copy(kvflat, kv_out, loc.at[15])
+    out_kv.start()
     for d in range(1, nt):
         sq2_copy(d).wait_recv()
         sq = sq + sq2_recv[d]
-    ssum = dot_hi(sq, jnp.full((8, oc), 0.125, F32), (((0,), (0,)), ((), ())))
+    ssum = dot_hi(jnp.broadcast_to(sq, (8, rows)), jnp.full((8, oc), 0.125, F32), (((0,), (0,)), ((), ())))
     mixed_out[...] = (mixed * lax.rsqrt(ssum / width + epsilon) * gpost[...]).astype(BF)
 
     def drain(d):
@@ -733,7 +761,8 @@
     each(nh, lambda e: rs2_copy(e).wait_send())
     gather_drain(3, q_view)
     gather_drain(4, att_view)
-    gather_drain(5, kv_view)
+    gather_drain(5, k_view)
+    gather_drain(11, v_view)
 
     def drain_t(d):
         o_copy(d).wait_send()
@@ -876,6 +905,8 @@
         scratch_shapes=[
             V((rows, width), BF),
             V((rows, width), BF),
+            V((rows, w_query.shape[0]), BF),
+            V((rows, 128), F32),
             V((1, width), F32),
             V((3,) + w_query.shape, BF),
             V(w_forget.T.shape, BF),
@@ -911,13 +942,13 @@
             V((rows, hw), BF),
             V((nt, rows, oc), BF),
             V((nt, rows, oc), BF),
-            V((8, rows), F32),
-            V((n, 8, rows), F32),
-            V((8, rows), F32),
-            V((nt, 8, rows), F32),
-            D((16,)),
-            D((11, n)),
-            D((11, n)),
+            V((1, rows), F32),
+            V((n, 1, rows), F32),
+            V((1, rows), F32),
+            V((nt, 1, rows), F32),
+            D((20,)),
+            D((12, n)),
+            D((12, n)),
             D((2, nt)),
             D((2, nt)),
         ],

time: 61.8 us -> 61.3 us (level)
  no operation moved by 1% of the time
where the time goes in v3:
time: 61.3 us; the launch traced here: 61.1 us
  Pallas kernels  60.5 us (99%)
  between operations  0.64 us (1%)
    pallas_call x1, Pallas kernels, fast_device(): pl.pallas_call(functools.partial(layer_kernel, n, nt, num_seqs, prop, hea...  56.2 us
    pallas_call x1, Pallas kernels, fast_device(): pl.pallas_call(functools.partial(write_kernel, num_seqs, prop, span), out...  4.34 us

profile of v3, /device:TPU:0, one launch (start us, length us, event | category | flops | bytes accessed | tf_op | source)
XLA Modules:
  0.0 61.1 jit_solution(14849619950982446966)
XLA Ops:
  0.6 56.2 %layer.1 = (bf16[256,128]{1,0:T(8,128)(2,1)}, bf16[2,1024,128]{2,1,0:T(8,128)(2,1)}, f32[64,128]{1,0:T(8,128)}) custom-call(bf16[256,4096]{1,0:T(8,128)(2,1)} %bitcast.16, f32[1,4096]{1,0:T(1,128)} %bitcast.20, bf16[512,512]{1,0:T(8,128)(2,1)} %wq.1, bf16[512,512]{1,0:T(8,128)(2,1)} %wk.1, bf16[512,512]{1,0:T(8,128)(2,1)} %wv.1, bf16[16,4096]{1,0:T(8,128)(2,1)} %bitcast.18, ...), custom_call_target="tpu_custom_call" | custom-call | tf_op jit(solution)/shard_map/layer/pallas_call | solution.py:896
  56.8 4.3 %cache_write.1 = (bf16[16,128,4,128]{3,2,1,0:T(4,128)(2,1)}, bf16[16,128,4,128]{3,2,1,0:T(4,128)(2,1)}, bf16[256,128]{1,0:T(8,128)(2,1)}, f32[64,128]{1,0:T(8,128)}) custom-call(bf16[16,128,4,128]{3,2,1,0:T(4,128)(2,1)} %kc.1, bf16[16,128,4,128]{3,2,1,0:T(4,128)(2,1)} %vc.1, bf16[2,16,16,4,128]{4,3,2,1,0:T(4,128)(2,1)} %bitcast.17, ...), custom_call_target="tpu_custom_call" | custom-call | tf_op jit(solution)/shard_map/cache_write/pallas_call | solution.py:976

commit v4 on v3

--- a/solution.py
+++ b/solution.py
@@ -339,7 +339,9 @@
         (wo, wov),
         (gpost_h, gpost),
     )
-    ins = [pltpu.make_async_copy(a, b, loc.at[i]) for i, (a, b) in enumerate(pairs)]
+    ins = [None] + [
+        pltpu.make_async_copy(a, b, loc.at[i]) for i, (a, b) in enumerate(pairs) if i > 0
+    ]
     pieces = 4
     piece = rows // pieces
     tok_in = [
@@ -497,6 +499,8 @@
         both_rows = jnp.dot(local, wv3[1 + i], preferred_element_type=F32).astype(BF)
         for c in range(n):
             part2[c % 2, c // 2, :, i * hw : (i + 1) * hw] = both_rows[c * R : (c + 1) * R]
+    rs1_copy().start()
+
     def norm_rest(i, c):
         sl = pl.ds(pl.multiple_of(i * nb, nb), nb)
         inv = invs[sl, 0:1]
@@ -568,7 +572,10 @@
         own_q = own_q + rsq[d].astype(F32)
     qall[rrow(me)] = own_q.astype(BF)
     gather_start(3, q_view)
-    rs1_copy().start()
+    rs1_copy().wait_recv()
+    for i in range(nh):
+        half[i] = (part2[par, i].astype(F32) + rs1[i].astype(F32)).astype(BF)
+    each(nh, lambda e: rs2_copy(e).start())
 
     ins[11].wait()
     ins[12].wait()
@@ -612,10 +619,6 @@
     val_recv[0] = values
     gather_pass(3, q_view)
     each(nh, lambda e: remote_block(2 * e))
-    rs1_copy().wait_recv()
-    for i in range(nh):
-        half[i] = (part2[par, i].astype(F32) + rs1[i].astype(F32)).astype(BF)
-    each(nh, lambda e: rs2_copy(e).start())
 
     def mate_block(e, c):
         gather_wait(3, e, q_view)
@@ -706,11 +709,11 @@
                 attended[j * hp + h * prop : j * hp + (h + 1) * prop]
             )
     gather_start(4, att_view)
-    gather_start(11, v_view)
     ins[13].wait()
     ins[14].wait()
+    gather_pass(4, att_view)
+    gather_start(11, v_view)
     gather_pass(5, k_view)
-    gather_pass(4, att_view)
     for e in range(nh):
         gather_wait(4, e, att_view)
     full = jnp.dot(att[...], wov[...], preferred_element_type=F32).astype(BF)

time: 61.3 us -> 59.7 us (0.974)
  Pallas kernels: 60.5 us -> 58.9 us
    pallas_call x1, Pallas kernels: 56.2 us -> 54.5 us  [fast_device(): pl.pallas_call(functools.partial(layer_kernel, n, nt, num_seqs, prop, hea...]
where the time goes in v4:
time: 59.7 us; the launch traced here: 59.5 us
  Pallas kernels  58.9 us (99%)
  between operations  0.64 us (1%)
    pallas_call x1, Pallas kernels, fast_device(): pl.pallas_call(functools.partial(layer_kernel, n, nt, num_seqs, prop, hea...  54.5 us
    pallas_call x1, Pallas kernels, fast_device(): pl.pallas_call(functools.partial(write_kernel, num_seqs, prop, span), out...  4.34 us

profile of v4, /device:TPU:0, one launch (start us, length us, event | category | flops | bytes accessed | tf_op | source)
XLA Modules:
  0.0 59.5 jit_solution(4284776575377777485)
XLA Ops:
  0.6 54.5 %layer.1 = (bf16[256,128]{1,0:T(8,128)(2,1)}, bf16[2,1024,128]{2,1,0:T(8,128)(2,1)}, f32[64,128]{1,0:T(8,128)}) custom-call(bf16[256,4096]{1,0:T(8,128)(2,1)} %bitcast.16, f32[1,4096]{1,0:T(1,128)} %bitcast.20, bf16[512,512]{1,0:T(8,128)(2,1)} %wq.1, bf16[512,512]{1,0:T(8,128)(2,1)} %wk.1, bf16[512,512]{1,0:T(8,128)(2,1)} %wv.1, bf16[16,4096]{1,0:T(8,128)(2,1)} %bitcast.18, ...), custom_call_target="tpu_custom_call" | custom-call | tf_op jit(solution)/shard_map/layer/pallas_call | solution.py:899
  55.2 4.3 %cache_write.1 = (bf16[16,128,4,128]{3,2,1,0:T(4,128)(2,1)}, bf16[16,128,4,128]{3,2,1,0:T(4,128)(2,1)}, bf16[256,128]{1,0:T(8,128)(2,1)}, f32[64,128]{1,0:T(8,128)}) custom-call(bf16[16,128,4,128]{3,2,1,0:T(4,128)(2,1)} %kc.1, bf16[16,128,4,128]{3,2,1,0:T(4,128)(2,1)} %vc.1, bf16[2,16,16,4,128]{4,3,2,1,0:T(4,128)(2,1)} %bitcast.17, ...), custom_call_target="tpu_custom_call" | custom-call | tf_op jit(solution)/shard_map/cache_write/pallas_call | solution.py:979

commit v5 on v4

--- a/solution.py
+++ b/solution.py
@@ -282,13 +282,13 @@
     o_recv,
     sq_send,
     sq_recv,
-    sq2_send,
-    sq2_recv,
     loc,
     ssem,
     rsem,
     tssem,
     trsem,
+    qssem,
+    qrsem,
 ):
     me = lax.axis_index("kv")
     mt = lax.axis_index("tp")
@@ -307,20 +307,18 @@
 
     barrier = pltpu.get_barrier_semaphore()
 
+    count = n * nt
+    spot = me * nt + mt
+
+    def place(d):
+        other = lax.rem(spot + d, count)
+        return {"kv": other // nt, "tp": lax.rem(other, nt)}
+
     def greet(d, c):
-        pl.semaphore_signal(
-            barrier, inc=1, device_id={"kv": lax.rem(me + d, n)}, device_id_type=MESH
-        )
+        pl.semaphore_signal(barrier, inc=1, device_id=place(d), device_id_type=MESH)
         return c
 
-    def greet_t(d, c):
-        pl.semaphore_signal(
-            barrier, inc=1, device_id={"tp": lax.rem(mt + d, nt)}, device_id_type=MESH
-        )
-        return c
-
-    lax.fori_loop(1, n, greet, 0)
-    lax.fori_loop(1, nt, greet_t, 0)
+    lax.fori_loop(1, count, greet, 0)
 
     pairs = (
         (tok, tokv),
@@ -463,14 +461,21 @@
         return to_kv(8, d, cand_send, cand_recv.at[d])
 
     def sq_copy(d):
-        return to_kv(10, d, sq_send, sq_recv.at[d])
-
-    def each(count, fn):
+        return pltpu.make_async_remote_copy(
+            src_ref=sq_send,
+            dst_ref=sq_recv.at[d],
+            send_sem=qssem.at[d],
+            recv_sem=qrsem.at[d],
+            device_id=place(d),
+            device_id_type=MESH,
+        )
+
+    def each(times, fn):
         def body(d, c):
             fn(d)
             return c
 
-        lax.fori_loop(1, count, body, 0)
+        lax.fori_loop(1, times, body, 0)
 
     nb = min(2 * prop, piece)
     mine = pl.ds(pl.multiple_of(me * kdim, kdim), kdim)
@@ -490,7 +495,7 @@
     for c in ins[5:]:
         c.start()
     local = slab[...]
-    pl.semaphore_wait(barrier, n - 1 + nt - 1)
+    pl.semaphore_wait(barrier, count - 1)
     ins[2].wait()
     partq[...] = jnp.dot(local, wv3[0], preferred_element_type=F32).astype(BF)
     each(n, lambda d: rsq_copy(d).start())
@@ -724,9 +729,6 @@
     def o_copy(d):
         return to_tp(0, d, o_send.at[lax.rem(mt + d, nt)], o_recv.at[d])
 
-    def sq2_copy(d):
-        return to_tp(1, d, sq2_send, sq2_recv.at[d])
-
     each(nt, lambda d: o_copy(d).start())
     gather_pass(11, v_view)
     mixed = o_send[mt].astype(F32)
@@ -734,21 +736,15 @@
         o_copy(d).wait_recv()
         mixed = mixed + o_recv[d].astype(F32)
     sq_send[...] = dot_hi(jnp.ones((8, oc), F32), mixed * mixed, NT)[0:1]
-    each(n, lambda d: sq_copy(d).start())
-    sq = sq_send[...]
-    for d in range(1, n):
-        sq_copy(d).wait_recv()
-        sq = sq + sq_recv[d]
-    sq2_send[...] = sq
-    each(nt, lambda d: sq2_copy(d).start())
+    each(count, lambda d: sq_copy(d).start())
     for e in range(nh):
         gather_wait(5, e, k_view)
         gather_wait(11, e, v_view)
     out_kv = pltpu.make_async_copy(kvflat, kv_out, loc.at[15])
     out_kv.start()
-    for d in range(1, nt):
-        sq2_copy(d).wait_recv()
-        sq = sq + sq2_recv[d]
+    each(count, lambda d: sq_copy(d).wait_recv())
+    sq_recv[0] = sq_send[...]
+    sq = jnp.sum(sq_recv[...], axis=0)
     ssum = dot_hi(jnp.broadcast_to(sq, (8, rows)), jnp.full((8, oc), 0.125, F32), (((0,), (0,)), ((), ())))
     mixed_out[...] = (mixed * lax.rsqrt(ssum / width + epsilon) * gpost[...]).astype(BF)
 
@@ -757,9 +753,9 @@
         stat_copy(d).wait_send()
         val_copy(d).wait_send()
         cand_copy(d).wait_send()
-        sq_copy(d).wait_send()
 
     each(n, drain)
+    each(count, lambda d: sq_copy(d).wait_send())
     rs1_copy().wait_send()
     each(nh, lambda e: rs2_copy(e).wait_send())
     gather_drain(3, q_view)
@@ -769,7 +765,6 @@
 
     def drain_t(d):
         o_copy(d).wait_send()
-        sq2_copy(d).wait_send()
 
     each(nt, drain_t)
     out_kv.wait()
@@ -946,14 +941,14 @@
             V((nt, rows, oc), BF),
             V((nt, rows, oc), BF),
             V((1, rows), F32),
-            V((n, 1, rows), F32),
-            V((1, rows), F32),
-            V((nt, 1, rows), F32),
+            V((n * nt, 1, rows), F32),
             D((20,)),
             D((12, n)),
             D((12, n)),
-            D((2, nt)),
-            D((2, nt)),
+            D((1, nt)),
+            D((1, nt)),
+            D((n * nt,)),
+            D((n * nt,)),
         ],
         compiler_params=pltpu.CompilerParams(
             collective_id=0, has_side_effects=True, vmem_limit_bytes=67043328

time: 59.7 us -> 59.9 us (level)
  no operation moved by 1% of the time
where the time goes in v5:
time: 59.9 us; the launch traced here: 59.7 us
  Pallas kernels  59.1 us (99%)
  between operations  0.64 us (1%)
    pallas_call x1, Pallas kernels, fast_device(): pl.pallas_call(functools.partial(layer_kernel, n, nt, num_seqs, prop, hea...  54.7 us
    pallas_call x1, Pallas kernels, fast_device(): pl.pallas_call(functools.partial(write_kernel, num_seqs, prop, span), out...  4.34 us

profile of v5, /device:TPU:0, one launch (start us, length us, event | category | flops | bytes accessed | tf_op | source)
XLA Modules:
  0.0 59.7 jit_solution(9069349508948134159)
XLA Ops:
  0.6 54.7 %layer.1 = (bf16[256,128]{1,0:T(8,128)(2,1)}, bf16[2,1024,128]{2,1,0:T(8,128)(2,1)}, f32[64,128]{1,0:T(8,128)}) custom-call(bf16[256,4096]{1,0:T(8,128)(2,1)} %bitcast.16, f32[1,4096]{1,0:T(1,128)} %bitcast.20, bf16[512,512]{1,0:T(8,128)(2,1)} %wq.1, bf16[512,512]{1,0:T(8,128)(2,1)} %wk.1, bf16[512,512]{1,0:T(8,128)(2,1)} %wv.1, bf16[16,4096]{1,0:T(8,128)(2,1)} %bitcast.18, ...), custom_call_target="tpu_custom_call" | custom-call | tf_op jit(solution)/shard_map/layer/pallas_call | solution.py:894
  55.4 4.3 %cache_write.1 = (bf16[16,128,4,128]{3,2,1,0:T(4,128)(2,1)}, bf16[16,128,4,128]{3,2,1,0:T(4,128)(2,1)}, bf16[256,128]{1,0:T(8,128)(2,1)}, f32[64,128]{1,0:T(8,128)}) custom-call(bf16[16,128,4,128]{3,2,1,0:T(4,128)(2,1)} %kc.1, bf16[16,128,4,128]{3,2,1,0:T(4,128)(2,1)} %vc.1, bf16[2,16,16,4,128]{4,3,2,1,0:T(4,128)(2,1)} %bitcast.17, ...), custom_call_target="tpu_custom_call" | custom-call | tf_op jit(solution)/shard_map/cache_write/pallas_call | solution.py:974
